TPU v7x, 32 devices: a whole 2x2x4 slice. The times are simulated.
32 devices in a mesh: sp: 16 (over z, y, x), tp: 2 (over core).
Axes of the slice: x: 2, y: 2, z: 4, core: 2. Of those that a mesh axis runs over, the one named last changes fastest.
Arguments:
- tokens: bfloat16 [4096, 2048], P('sp'), may hold values from -6 to 6
- input_norm_gain: float32 [2048], replicated, may hold values from 0.1 to 1.9
- mq_weight: bfloat16 [2048, 1024], P('sp', 'tp'), may hold values from -0.125 to 0.125
- mk_weight: bfloat16 [2048, 1024], P('sp', 'tp'), may hold values from -0.125 to 0.125
- mv_weight: bfloat16 [2048, 1024], P('sp', 'tp'), may hold values from -0.125 to 0.125
- mo_weight: bfloat16 [2048, 1024], P('sp', 'tp'), may hold values from -0.125 to 0.125
- gate_weight: bfloat16 [2048, 4, 8], P('sp', None, 'tp'), may hold values from -0.125 to 0.125
- gate_bias: float32 [4, 8], P(None, 'tp'), may hold values from -3 to 100
- decay_extra: float32 [2, 8, 4096], P(None, 'tp', 'sp'), may hold values from -1 to 0
- m_gain: float32 [1024], P('tp'), may hold values from 0.1 to 1.9
- aq_weight: bfloat16 [2048, 1024], P('sp', 'tp'), may hold values from -0.125 to 0.125
- ak_weight: bfloat16 [2048, 512], P('sp', 'tp'), may hold values from -8.838835 to 8.838835
- av_weight: bfloat16 [2048, 512], P('sp', 'tp'), may hold values from -0.125 to 0.125
- sink_logit: float32 [16], P('tp'), may hold values from 3 to 6
- out_m_weight: bfloat16 [1024, 2048], P('sp', 'tp'), may hold values from -0.1875 to 0.1875
- out_a_weight: bfloat16 [1024, 2048], P('sp', 'tp'), may hold values from -1.5 to 1.5
Outputs:
- mixed: bfloat16 [4096, 2048], P('sp', 'tp')
- log_total: float32 [16, 4096], P('tp', 'sp')
All inputs are finite; a program needn't handle non-finite values.
Results may differ from a plain program's by a relative error of at most 0.015.
The roundings to bfloat16 on the way count: a program that leaves them out, or rounds other values in their place, can miss the bound.
Values may be sent and summed in bfloat16 or wider, within the bound.
A program may use at most 64 MiB of HBM per device.

v0:
```python
import jax
import jax.numpy as jnp
from jax import lax
from jax.sharding import PartitionSpec as P

M_DIM = 128
W_DIM = 64
WINDOW = 128
M_BLOCK = 64


EPS = 1e-06
FLOOR_LOG = -1e30
HIGHEST = lax.Precision.HIGHEST


def with_halo(x, sides, width):
    for axis, dim in sides:
        peers, length = (lax.axis_size(axis), x.shape[dim])
        up = [(i, (i + 1) % peers) for i in range(peers - 1)]
        down = [(j, i) for i, j in up]
        last = lax.slice_in_dim(x, length - width, length, axis=dim)
        first = lax.slice_in_dim(x, 0, width, axis=dim)
        before = lax.ppermute(last, axis, up)
        after = lax.ppermute(first, axis, down)
        x = jnp.concatenate([before, x, after], axis=dim)
    return x


def rms_rows(inputs, gain_vec):
    return inputs * lax.rsqrt(jnp.mean(inputs * inputs, axis=-1, keepdims=True) + EPS) * gain_vec


def stored(result):
    return lax.optimization_barrier(result.astype(jnp.bfloat16))


def flip_tokens(array_in):
    return jnp.flip(array_in, axis=1)


def block_pass(queries, key_vecs, value_vecs, in_gate, log_forget, start_state):
    head_count, length, head_width = queries.shape
    block_count = length // M_BLOCK

    def blocks(array_in):
        return jnp.moveaxis(
            array_in.reshape((head_count, block_count, M_BLOCK) + array_in.shape[2:]), 1, 0
        )

    lower_mask = jnp.tril(jnp.ones((M_BLOCK, M_BLOCK), dtype=bool))

    def advance(state_in, block_in):
        cell_mat, norm_vec, stab_max = state_in
        q_blk, k_blk, v_blk, i_blk, f_blk = block_in
        cum_log = jnp.cumsum(f_blk, axis=-1)
        seg_total = cum_log[:, -1]
        log_end = seg_total[:, None] - cum_log + i_blk
        max_next = jnp.maximum(seg_total + stab_max, jnp.max(log_end, axis=-1))
        w_end = jnp.exp(log_end - max_next[:, None])
        fade_old = jnp.exp(seg_total + stab_max - max_next)
        cell_next = fade_old[:, None, None] * cell_mat + jnp.einsum(
            "hsv,hsk->hvk", w_end[:, :, None] * v_blk, k_blk, precision=HIGHEST
        )
        norm_next = fade_old[:, None] * norm_vec + jnp.einsum(
            "hs,hsk->hk", w_end, k_blk, precision=HIGHEST
        )
        log_w = jnp.where(
            lower_mask, cum_log[:, :, None] - cum_log[:, None, :] + i_blk[:, None, :], -jnp.inf
        )
        log_inter = cum_log + stab_max[:, None]
        row_max = jnp.maximum(log_inter, jnp.max(log_w, axis=-1))
        w_intra = jnp.exp(log_w - row_max[:, :, None])
        w_inter = jnp.exp(log_inter - row_max)
        scores = jnp.einsum("htk,hsk->hts", q_blk, k_blk, precision=HIGHEST) * w_intra
        numerator = jnp.einsum("hts,hsv->htv", scores, v_blk, precision=HIGHEST) + w_inter[
            ..., None
        ] * jnp.einsum("hvk,htk->htv", cell_mat, q_blk, precision=HIGHEST)
        denominator = jnp.sum(scores, axis=-1) + w_inter * jnp.einsum(
            "hk,htk->ht", norm_vec, q_blk, precision=HIGHEST
        )
        result_rows = numerator / jnp.maximum(jnp.abs(denominator), jnp.exp(-row_max))[..., None]
        return ((cell_next, norm_next, max_next), result_rows)

    final_state, outputs = lax.scan(
        advance,
        start_state,
        tuple(
            (blocks(array_in) for array_in in (queries, key_vecs, value_vecs, in_gate, log_forget))
        ),
    )
    return (jnp.moveaxis(outputs, 0, 1).reshape(head_count, length, head_width), final_state)


def summarize(key_vecs, value_vecs, in_gate, log_forget):
    cum_log = jnp.cumsum(log_forget, axis=-1)
    seg_total = cum_log[:, -1]
    log_end = seg_total[:, None] - cum_log + in_gate
    peak_log = jnp.max(log_end, axis=-1)
    weights_end = jnp.exp(log_end - peak_log[:, None])
    cell_mat = jnp.einsum(
        "hsv,hsk->hvk", weights_end[:, :, None] * value_vecs, key_vecs, precision=HIGHEST
    )
    norm_vec = jnp.einsum("hs,hsk->hk", weights_end, key_vecs, precision=HIGHEST)
    return (seg_total, cell_mat, norm_vec, peak_log)


def merge_side(state_in, cell_mats, norm_vecs, logs, usable):
    cell_mat, norm_vec, peak_log = state_in
    masked = jnp.where(usable, logs, FLOOR_LOG)
    new_peak = jnp.maximum(peak_log, jnp.max(masked, axis=0))
    scales = jnp.where(usable, jnp.exp(masked - new_peak[None]), 0.0)
    cell_mat = jnp.einsum("jh,jhvk->hvk", scales, cell_mats, precision=HIGHEST)
    norm_vec = jnp.einsum("jh,jhk->hk", scales, norm_vecs, precision=HIGHEST)
    return (cell_mat, norm_vec, new_peak)


def gather_states(forward_sum, backward_sum):
    decay_all = (
        lax.all_gather(forward_sum[0][None], "sp", axis=0, tiled=True),
        lax.all_gather(backward_sum[0][None], "sp", axis=0, tiled=True),
    )
    own_index = lax.axis_index("sp")
    acc_fwd = jnp.cumsum(decay_all[0], axis=0)
    acc_bwd = jnp.cumsum(decay_all[1], axis=0)
    before_own = lax.dynamic_index_in_dim(acc_fwd - decay_all[0], own_index, 0, keepdims=False)
    after_own = lax.dynamic_index_in_dim(acc_bwd, own_index, 0, keepdims=False)
    lead_bwd = acc_bwd - decay_all[1]
    empty_side = (
        jnp.zeros_like(forward_sum[1]),
        jnp.zeros_like(forward_sum[2]),
        jnp.full_like(forward_sum[3], FLOOR_LOG),
    )
    state_in = empty_side + empty_side
    pieces = (
        lax.all_gather(forward_sum[1][None], "sp", axis=0, tiled=True),
        lax.all_gather(forward_sum[2][None], "sp", axis=0, tiled=True),
        lax.all_gather(forward_sum[3][None], "sp", axis=0, tiled=True),
        lax.all_gather(backward_sum[1][None], "sp", axis=0, tiled=True),
        lax.all_gather(backward_sum[2][None], "sp", axis=0, tiled=True),
        lax.all_gather(backward_sum[3][None], "sp", axis=0, tiled=True),
    )
    piece_count = pieces[0].shape[0]
    device_ids = jnp.arange(piece_count, dtype=jnp.int32)
    log_fwd = before_own[None] - acc_fwd + pieces[2]
    log_bwd = lead_bwd - after_own[None] + pieces[5]
    left_side = merge_side(
        state_in[:3], pieces[0], pieces[1], log_fwd, (device_ids < own_index)[:, None]
    )
    right_side = merge_side(
        state_in[3:], pieces[3], pieces[4], log_bwd, (device_ids > own_index)[:, None]
    )
    states = left_side + right_side
    return (states[:3], states[3:])


def window_attend(a_query, kv_pairs, sink_logit, first_row, total_rows):
    tok_rows = a_query.shape[0]
    block_len = WINDOW
    block_count = tok_rows // block_len
    kv_width = kv_pairs.shape[1] // 2
    kv_heads = kv_width // W_DIM
    q_heads = a_query.shape[1] // W_DIM
    groups = q_heads // kv_heads
    filled_margin = with_halo(kv_pairs, (("sp", 0),), WINDOW)
    windows = jnp.concatenate(
        [
            filled_margin[place_idx * block_len : place_idx * block_len + tok_rows].reshape(
                block_count, block_len, 2 * kv_width
            )
            for place_idx in range(3)
        ],
        axis=1,
    )
    key_block = windows[:, :, :kv_width].reshape(block_count, 3 * block_len, kv_heads, W_DIM)
    content_tile = windows[:, :, kv_width:].reshape(block_count, 3 * block_len, kv_heads, W_DIM)
    query_block = a_query.reshape(block_count, block_len, kv_heads, groups, W_DIM)
    scores = jnp.einsum(
        "nqgrd,nkgd->ngrqk", query_block, key_block, preferred_element_type=jnp.float32
    ) * W_DIM ** (-0.5)
    query_off = jnp.arange(block_len, dtype=jnp.int32)
    key_off = jnp.arange(3 * block_len, dtype=jnp.int32) - block_len
    in_window = jnp.abs(query_off[:, None] - key_off[None, :]) <= WINDOW
    key_place = (
        first_row + jnp.arange(block_count, dtype=jnp.int32)[:, None] * block_len + key_off[None, :]
    )
    inside = (key_place >= 0) & (key_place < total_rows)
    usable = in_window[None] & inside[:, None, :]
    scores = jnp.where(usable[:, None, None], scores, -jnp.inf)
    sink_col = sink_logit.reshape(kv_heads, groups)[None, :, :, None]
    peak_log = jnp.maximum(sink_col, jnp.max(scores, axis=-1))
    weights_exp = jnp.exp(scores - peak_log[..., None])
    weight_total_sum = jnp.exp(sink_col - peak_log) + jnp.sum(weights_exp, axis=-1)
    weighted = jnp.einsum(
        "ngrqk,nkgd->nqgrd",
        weights_exp.astype(jnp.bfloat16),
        content_tile,
        preferred_element_type=jnp.float32,
    )
    scale_back = jnp.transpose(weight_total_sum, (0, 3, 1, 2))[..., None]
    mixed_rows = (weighted / scale_back).astype(jnp.bfloat16).reshape(tok_rows, q_heads * W_DIM)
    log_total = jnp.transpose(peak_log + jnp.log(weight_total_sum), (1, 2, 0, 3)).reshape(
        q_heads, tok_rows
    )
    return (mixed_rows, log_total)


def on_device(
    tokens,
    input_norm_gain,
    mq_weight,
    mk_weight,
    mv_weight,
    mo_weight,
    gate_weight,
    gate_bias,
    decay_extra,
    m_gain,
    aq_weight,
    ak_weight,
    av_weight,
    sink_logit,
    out_m_weight,
    out_a_weight,
):
    tok_rows = tokens.shape[0]
    normed = rms_rows(tokens.astype(jnp.float32), input_norm_gain).astype(jnp.bfloat16)
    local_heads = gate_weight.shape[2]
    gate_cols = 4 * local_heads
    pieces = (
        lax.all_gather(mq_weight, "sp", axis=0, tiled=True),
        lax.all_gather(mk_weight, "sp", axis=0, tiled=True),
        lax.all_gather(mv_weight, "sp", axis=0, tiled=True),
        lax.all_gather(mo_weight, "sp", axis=0, tiled=True),
        lax.all_gather(gate_weight, "sp", axis=0, tiled=True),
        lax.all_gather(aq_weight, "sp", axis=0, tiled=True),
        lax.all_gather(ak_weight, "sp", axis=0, tiled=True),
        lax.all_gather(av_weight, "sp", axis=0, tiled=True),
    )
    piece_rows = pieces[0].shape[0]
    flat_gate = pieces[4].reshape(piece_rows, gate_cols)
    segments = (
        pieces[0],
        pieces[1],
        pieces[2],
        pieces[3],
        flat_gate,
        pieces[5],
        pieces[6],
        pieces[7],
    )
    projected = tuple(
        (jnp.dot(normed, segment, preferred_element_type=jnp.float32) for segment in segments)
    )
    m_query = stored(projected[0])
    m_key = stored(projected[1])
    m_value = stored(projected[2])
    m_out = stored(projected[3])
    gates = projected[4].reshape(tok_rows, 4, local_heads) + gate_bias[None]

    def heads_first(matrix):
        return jnp.transpose(
            matrix.astype(jnp.float32).reshape(tok_rows, local_heads, M_DIM), (1, 0, 2)
        )

    queries = heads_first(m_query)
    key_vecs = heads_first(m_key) * M_DIM ** (-0.5)
    value_vecs = heads_first(m_value)
    in_fwd = gates[:, 0, :].T
    forget_fwd = jax.nn.log_sigmoid(gates[:, 1, :].T) + decay_extra[0]
    in_bwd = flip_tokens(gates[:, 2, :].T)
    forget_bwd = flip_tokens(jax.nn.log_sigmoid(gates[:, 3, :].T) + decay_extra[1])
    queries_bwd = flip_tokens(queries)
    keys_bwd = flip_tokens(key_vecs)
    values_bwd = flip_tokens(value_vecs)
    forward_sum = summarize(key_vecs, value_vecs, in_fwd, forget_fwd)
    backward_sum = summarize(keys_bwd, values_bwd, in_bwd, forget_bwd)
    state_fwd, state_bwd = gather_states(forward_sum, backward_sum)
    hidden_fwd, forward_unused = block_pass(
        queries, key_vecs, value_vecs, in_fwd, forget_fwd, state_fwd
    )
    hidden_bwd, unused_bwd = block_pass(
        queries_bwd, keys_bwd, values_bwd, in_bwd, forget_bwd, state_bwd
    )
    cell_out = hidden_fwd + flip_tokens(hidden_bwd)
    gate_open = jax.nn.sigmoid(m_out.astype(jnp.float32)).reshape(tok_rows, local_heads, M_DIM)
    cell_rows = jnp.transpose(cell_out, (1, 0, 2)) * gate_open
    mixed_m = (
        rms_rows(cell_rows, m_gain.reshape(local_heads, M_DIM))
        .astype(jnp.bfloat16)
        .reshape(tok_rows, local_heads * M_DIM)
    )
    a_query = stored(projected[5])
    kv_pairs = jnp.concatenate([stored(projected[6]), stored(projected[7])], axis=1)
    first_row = lax.axis_index("sp") * tok_rows
    total_rows = tok_rows * lax.axis_size("sp")
    mixed_a, log_total = window_attend(a_query, kv_pairs, sink_logit, first_row, total_rows)
    full_m, full_a = (
        lax.all_gather(mixed_m, "tp", axis=1, tiled=True),
        lax.all_gather(mixed_a, "tp", axis=1, tiled=True),
    )
    pieces = (
        lax.all_gather(out_m_weight, "sp", axis=0, tiled=True),
        lax.all_gather(out_a_weight, "sp", axis=0, tiled=True),
    )
    running = jnp.dot(full_m, pieces[0], preferred_element_type=jnp.float32)
    mixed = running + jnp.dot(full_a, pieces[1], preferred_element_type=jnp.float32)
    return (mixed.astype(jnp.bfloat16), log_total)


def solution(mesh):
    in_specs = (
        P("sp", None),
        P(),
        P("sp", "tp"),
        P("sp", "tp"),
        P("sp", "tp"),
        P("sp", "tp"),
        P("sp", None, "tp"),
        P(None, "tp"),
        P(None, "tp", "sp"),
        P("tp"),
        P("sp", "tp"),
        P("sp", "tp"),
        P("sp", "tp"),
        P("tp"),
        P("sp", "tp"),
        P("sp", "tp"),
    )
    out_specs = (P("sp", "tp"), P("tp", "sp"))
    return jax.shard_map(
        on_device, mesh=mesh, in_specs=in_specs, out_specs=out_specs, check_vma=False
    )
```

profile of v0, /device:TPU:0, one launch (start us, length us, event | category | flops | bytes accessed | tf_op | source)
XLA Modules:
  0.0 723.0 jit_solution(17199120740236358637)
XLA Ops:
  12.0 43.3 %all_gather.60 = bf16[2048,4,4]{0,2,1:T(4,128)(2,1)S(1)} all-gather(bf16[128,4,4]{0,2,1:T(4,128)(2,1)} %param.26), channel_id=1, replica_groups=mesh['sp'=16,'tp'=2] {'sp'}, dimensions={0}, use_global_device_ids=true | all-gather | bytes 69632 | tf_op jit(solution)/shard_map/all_gather | solution.py:235
  55.3 1.5 fusion.73
  57.4 1.2 reduce-window.14
  59.4 14.5 %all-gather.22.cloned.1.call-done = bf16[2048,512]{1,0:T(8,128)(2,1)} async-done(((bf16[128,512]{1,0:T(8,128)(2,1)}), bf16[2048,512]{1,0:T(8,128)(2,1)}) %all-gather.22.cloned.1.call-update) | async-done | bytes 2097168 | tf_op jit(solution)/shard_map/all_gather | solution.py:233
  74.0 2.3 convolution_convert_fusion.4
  76.3 59.6 %all-gather.24.cloned.1.call-done = bf16[2048,512]{1,0:T(8,128)(2,1)} async-done(((bf16[128,512]{1,0:T(8,128)(2,1)}), bf16[2048,512]{1,0:T(8,128)(2,1)}) %all-gather.24.cloned.1.call-update) | async-done | bytes 2097168 | tf_op jit(solution)/shard_map/all_gather | solution.py:232
  135.9 2.3 convolution_convert_fusion.3
  138.4 1.9 fusion.94
  140.6 1.2 reduce-window.16
  143.5 1.9 fusion.92
  149.4 39.7 %all-reduce.4 = (f32[64]{0:T(128)S(1)}, f32[64]{0:T(128)S(1)}, f32[64]{0:T(128)S(1)}, f32[64]{0:T(128)S(1)}) all-reduce(f32[64]{0:T(128)S(1)} %dynamic-update-slice.3, f32[64]{0:T(128)S(1)} %dynamic-update-slice.2, f32[64]{0:T(128)S(1)} %dynamic-update-slice.1, f32[64]{0:T(128)S(1)} %dynamic-update-slice), channel_id=7, replica_groups=mesh['sp'=16,'tp'=2] {'sp'}, use_global_device_ids=true, to_apply=%add.3 | all-reduce | flops 256 | bytes 2048
  192.9 2.0 convolution_convert_fusion.6
  194.9 54.5 %all-gather.34.cloned.1.call-done = bf16[2048,256]{1,0:T(8,128)(2,1)} async-done(((bf16[128,256]{1,0:T(8,128)(2,1)}), bf16[2048,256]{1,0:T(8,128)(2,1)}) %all-gather.34.cloned.1.call-update) | async-done | bytes 1048592 | tf_op jit(solution)/shard_map/all_gather | solution.py:238
  249.5 2.0 convolution_convert_fusion.5
  251.5 3.4 collective-permute-start
  254.9 1.5 collective-permute-start.1
  256.4 2.4 collective-permute-done
  258.8 3.0 collective-permute-done.1
  262.2 0.9 copy.123
  263.1 48.2 %all-gather.36.cloned.1.call-done = bf16[2048,512]{1,0:T(8,128)(2,1)} async-done(((bf16[128,512]{1,0:T(8,128)(2,1)}), bf16[2048,512]{1,0:T(8,128)(2,1)}) %all-gather.36.cloned.1.call-update) | async-done | bytes 2097168 | tf_op jit(solution)/shard_map/all_gather | solution.py:236
  311.3 2.7 convolution_convert_fusion
  314.3 0.7 fusion.72
  316.6 0.9 fusion.86
  317.8 2.3 all_gather.78
  320.5 38.8 %all-gather.8 = f32[16,4,128]{2,1,0:T(4,128)S(1)} all-gather(f32[1,4,128]{2,1,0:T(4,128)S(1)} %bitcast.480), channel_id=5, replica_groups=mesh['sp'=16,'tp'=2] {'sp'}, dimensions={0}, use_global_device_ids=true | all-gather | bytes 34816 | tf_op jit(solution)/shard_map/all_gather | solution.py:137
  359.3 13.9 %all-gather.26.cloned.1.call-done = bf16[2048,512]{1,0:T(8,128)(2,1)} async-done(((bf16[128,512]{1,0:T(8,128)(2,1)}), bf16[2048,512]{1,0:T(8,128)(2,1)}) %all-gather.26.cloned.1.call-update) | async-done | bytes 2097168 | tf_op jit(solution)/shard_map/all_gather | solution.py:231
  373.2 2.7 convolution_convert_fusion.2
  375.9 0.9 copy_bitcast_fusion
  377.2 38.9 %all-gather.9 = f32[16,4,128]{2,1,0:T(4,128)S(1)} all-gather(f32[1,4,128]{2,1,0:T(4,128)S(1)} %bitcast.481), channel_id=9, replica_groups=mesh['sp'=16,'tp'=2] {'sp'}, dimensions={0}, use_global_device_ids=true | all-gather | bytes 34816 | tf_op jit(solution)/shard_map/all_gather | solution.py:140
  416.1 3.4 rev.24
  419.6 15.7 %all-gather.28.cloned.1.call-done = bf16[2048,512]{1,0:T(8,128)(2,1)} async-done(((bf16[128,512]{1,0:T(8,128)(2,1)}), bf16[2048,512]{1,0:T(8,128)(2,1)}) %all-gather.28.cloned.1.call-update) | async-done | bytes 2097168 | tf_op jit(solution)/shard_map/all_gather | solution.py:234
  435.3 3.4 convolution_convert_fusion.1
  439.0 73.5 %all-gather.40.cloned.1.call-done = f32[64,128,128]{2,1,0:T(8,128)} async-done(((f32[4,128,128]{2,1,0:T(8,128)}), f32[64,128,128]{2,1,0:T(8,128)}) %all-gather.40.cloned.1.call-update) | async-done | bytes 4194320 | tf_op jit(solution)/shard_map/all_gather | solution.py:136
  512.5 6.4 fusion.68
  518.9 0.8 broadcast.249.clone2.1
  519.8 17.3 %while.34 = (s32[]{:T(128)}, f32[4,128,128]{2,1,0:T(8,128)S(1)}, f32[4,128]{1,0:T(4,128)S(1)}, f32[4]{0:T(128)S(1)}, f32[4,4,64,128]{3,2,0,1:T(8,128)}, /*index=...) while((s32[]{:T(128)}, f32[4,128,128]{2,1,0:T(8,128)S(1)}, ...), condition=%wide.region_11.12_spmd.clone, body=%wide.region_6.11_spmd.clone.sunk | while | flops 152231936 | bytes 2495373 | solution.py:85
  521.8 1.3 fusion.218
  526.1 1.3 fusion.218
  530.5 1.3 fusion.218
  534.8 1.3 fusion.218
  537.1 52.6 %all-gather.42.cloned.1.call-done = f32[64,128,128]{2,1,0:T(8,128)} async-done(((f32[4,128,128]{2,1,0:T(8,128)}), f32[64,128,128]{2,1,0:T(8,128)}) %all-gather.42.cloned.1.call-update) | async-done | bytes 4194320 | tf_op jit(solution)/shard_map/all_gather | solution.py:139
  589.7 6.4 fusion.66
  596.2 15.0 %while.35 = (s32[]{:T(128)}, f32[4,128,128]{2,1,0:T(8,128)S(1)}, f32[4,128]{1,0:T(4,128)S(1)}, f32[4]{0:T(128)S(1)}, f32[4,4,64,128]{3,2,0,1:T(8,128)S(1)}, /*in...) while((s32[]{:T(128)}, f32[4,128,128]{2,1,0:T(8,128)S(1)}, ...), condition=%wide.region_22.23_spmd.clone, body=%wide.region_17.22_spmd.clone.sunk | while | flops 152231936 | bytes 2495373 | solution.py:85
  612.8 2.3 all_gather.73
  615.1 36.2 %all-gather.30.cloned.1.call-done = bf16[1024,1024]{1,0:T(8,128)(2,1)} async-done(((bf16[64,1024]{1,0:T(8,128)(2,1)}), bf16[1024,1024]{1,0:T(8,128)(2,1)}) %all-gather.30.cloned.1.call-update) | async-done | bytes 2097168 | tf_op jit(solution)/shard_map/all_gather | solution.py:303
  651.3 2.3 fusion.144
  653.6 59.7 %all-gather.38.cloned.1.call-done = bf16[1024,1024]{1,0:T(8,128)(2,1)} async-done(((bf16[64,1024]{1,0:T(8,128)(2,1)}), bf16[1024,1024]{1,0:T(8,128)(2,1)}) %all-gather.38.cloned.1.call-update) | async-done | bytes 2097168 | tf_op jit(solution)/shard_map/all_gather | solution.py:304
  713.3 3.1 fusion.79
  (304 shorter events, 47.0 us)
Async XLA Ops:
  7.2 49.6 %copy-start.4 = (bf16[256,2048]{1,0:T(8,128)(2,1)S(1)}, bf16[256,2048]{1,0:T(8,128)(2,1)}, u32[]{:S(2)}) copy-start(bf16[256,2048]{1,0:T(8,128)(2,1)} %param.20) | copy-start | bytes 3145732
  7.2 49.6 %copy-start.19 = (f32[2048]{0:T(1024)S(1)}, f32[2048]{0:T(1024)}, u32[]{:S(2)}) copy-start(f32[2048]{0:T(1024)} %param.21) | copy-start | bytes 24580
  7.2 49.6 %copy-start.22 = (f32[4,4]{1,0:T(4,128)S(1)}, f32[4,4]{1,0:T(4,128)}, u32[]{:S(2)}) copy-start(f32[4,4]{1,0:T(4,128)} %param.27) | copy-start | bytes 196
  7.2 66.8 %all-gather.22.cloned.1.call-start = ((), (), s32[]{:S(2)}) async-start(), calls=%async_computation | async-start | bytes 2228224 | tf_op jit(solution)/shard_map/all_gather | solution.py:233
  7.9 128.0 %all-gather.24.cloned.1.call-start = ((), (), s32[]{:S(2)}) async-start(), calls=%async_computation.1 | async-start | bytes 2228224 | tf_op jit(solution)/shard_map/all_gather | solution.py:232
  8.7 48.6 %copy-start.11 = (f32[2,4,256]{2,1,0:T(4,128)S(1)}, f32[2,4,256]{2,1,0:T(4,128)}, u32[]{:S(2)}) copy-start(f32[2,4,256]{2,1,0:T(4,128)} %param.28) | copy-start | bytes 24580
  8.7 184.2 %all-gather.32.cloned.1.call-start = ((), (), s32[]{:S(2)}) async-start(), calls=%async_computation.5 | async-start | bytes 1114112 | tf_op jit(solution)/shard_map/all_gather | solution.py:237
  9.4 240.0 %all-gather.34.cloned.1.call-start = ((), (), s32[]{:S(2)}) async-start(), calls=%async_computation.6 | async-start | bytes 1114112 | tf_op jit(solution)/shard_map/all_gather | solution.py:238
  10.0 301.3 %all-gather.36.cloned.1.call-start = ((), (), s32[]{:S(2)}) async-start(), calls=%async_computation.7 | async-start | bytes 2228224 | tf_op jit(solution)/shard_map/all_gather | solution.py:236
  10.6 362.6 %all-gather.26.cloned.1.call-start = ((), (), s32[]{:S(2)}) async-start(), calls=%async_computation.2 | async-start | bytes 2228224 | tf_op jit(solution)/shard_map/all_gather | solution.py:231
  11.2 424.1 %all-gather.28.cloned.1.call-start = ((), (), s32[]{:S(2)}) async-start(), calls=%async_computation.3 | async-start | bytes 2228224 | tf_op jit(solution)/shard_map/all_gather | solution.py:234
  11.9 500.6 %all-gather.40.cloned.1.call-start = ((), (), s32[]{:S(2)}) async-start(), calls=%async_computation.9 | async-start | bytes 4456448 | tf_op jit(solution)/shard_map/all_gather | solution.py:136
  56.8 192.6 %copy-start.15 = (f32[256]{0:T(256)}, f32[256]{0:T(256)S(1)}, u32[]{:S(2)}) copy-start(f32[256]{0:T(256)S(1)} %add_rsqrt_fusion.1) | copy-start | bytes 3076
  140.3 449.3 %all-gather.42.cloned.1.call-start = ((), (), s32[]{:S(2)}) async-start(), calls=%async_computation.10 | async-start | bytes 4456448 | tf_op jit(solution)/shard_map/all_gather | solution.py:139
  142.8 0.6 copy-start.7
  142.9 4.3 copy-start.18
  142.9 4.4 copy-start.23
  143.2 173.3 %copy-start = (f32[4,256,128]{2,1,0:T(8,128)}, f32[4,256,128]{2,1,0:T(8,128)S(1)}, u32[]{:S(2)}) copy-start(f32[4,256,128]{2,1,0:T(8,128)S(1)} %reverse.3) | copy-start | bytes 1572868
  145.4 505.9 %all-gather.30.cloned.1.call-start = ((), (), s32[]{:S(2)}) async-start(), calls=%async_computation.4 | async-start | bytes 2228224 | tf_op jit(solution)/shard_map/all_gather | solution.py:303
  146.0 567.3 %all-gather.38.cloned.1.call-start = ((), (), s32[]{:S(2)}) async-start(), calls=%async_computation.8 | async-start | bytes 2228224 | tf_op jit(solution)/shard_map/all_gather | solution.py:304
  251.5 7.3 %collective-permute-start = (bf16[128,512]{1,0:T(8,128)(2,1)S(1)}, bf16[128,512]{1,0:T(8,128)(2,1)S(1)}, u32[]{:S(2)}, u32[]{:S(2)}) collective-permute-start(bf16[128,512]{1,0:T(8,128)(2,1)S(1)} %get-tuple-element.297), channel_id=1, source_target_pairs={{0,2},{2,4},{4,6},{6,8},{8,10},{10,12},{12,14},{14,16},{16,18},{18... | collective-permute-start | bytes 393224 | tf_op jit(solution)/shard_map/ppermute | solution.py:24
  254.9 6.9 collective-permute-start.1
  261.9 49.4 %copy-start.16 = (f32[256]{0:T(256)S(1)}, f32[256]{0:T(256)}, u32[]{:S(2)}) copy-start(f32[256]{0:T(256)} %copy-done.15) | copy-start | bytes 3076
  261.9 49.4 %copy-start.20 = (f32[2048]{0:T(1024)S(1)}, f32[2048]{0:T(1024)}, u32[]{:S(2)}) copy-start(f32[2048]{0:T(1024)} %param.21) | copy-start | bytes 24580
  315.0 1.6 copy-start.6
  317.5 55.8 %copy-start.17 = (f32[256]{0:T(256)S(1)}, f32[256]{0:T(256)}, u32[]{:S(2)}) copy-start(f32[256]{0:T(256)} %copy-done.15) | copy-start | bytes 3076
  317.5 55.8 %copy-start.21 = (f32[2048]{0:T(1024)S(1)}, f32[2048]{0:T(1024)}, u32[]{:S(2)}) copy-start(f32[2048]{0:T(1024)} %param.21) | copy-start | bytes 24580
  359.3 17.5 %copy-start.1 = (f32[4,256,128]{2,1,0:T(8,128)S(1)}, f32[4,256,128]{2,1,0:T(8,128)}, u32[]{:S(2)}) copy-start(f32[4,256,128]{2,1,0:T(8,128)} %copy-done) | copy-start | bytes 1572868
  359.3 17.5 %copy-start.8 = (f32[4,256]{1,0:T(4,128)S(1)}, f32[4,256]{1,0:T(4,128)}, u32[]{:S(2)}) copy-start(f32[4,256]{1,0:T(4,128)} %copy-done.7) | copy-start | bytes 12292
  419.6 19.1 %copy-start.12 = (f32[16,4,1]{0,2,1:T(1,128)S(1)}, f32[16,4,1]{0,2,1:T(1,128)}, u32[]{:S(2)}) copy-start(f32[16,4,1]{0,2,1:T(1,128)} %copy.146) | copy-start | bytes 772
  419.6 19.3 %copy-start.13 = (f32[16,4,1]{0,2,1:T(1,128)S(1)}, f32[16,4,1]{0,2,1:T(1,128)}, u32[]{:S(2)}) copy-start(f32[16,4,1]{0,2,1:T(1,128)} %copy.155) | copy-start | bytes 772
  419.6 92.9 %copy-start.10 = (f32[16,4,1,1]{0,2,3,1:T(1,128)S(1)}, f32[16,4,1,1]{0,2,3,1:T(1,128)}, u32[]{:S(2)}) copy-start(f32[16,4,1,1]{0,2,3,1:T(1,128)} %copy.141) | copy-start | bytes 772
  519.8 69.9 %copy-start.9 = (f32[16,4,1,1]{0,2,3,1:T(1,128)S(1)}, f32[16,4,1,1]{0,2,3,1:T(1,128)}, u32[]{:S(2)}) copy-start(f32[16,4,1,1]{0,2,3,1:T(1,128)} %copy.150) | copy-start | bytes 772
  596.1 15.3 %copy-start.2 = (f32[4,4,64,128]{3,2,0,1:T(8,128)S(1)}, f32[4,4,64,128]{3,2,0,1:T(8,128)}, u32[]{:S(2)}) copy-start(f32[4,4,64,128]{3,2,0,1:T(8,128)} %get-tuple-element.116) | copy-start | bytes 1572868
  611.2 1.0 copy-start.5
  611.2 1.2 copy-start.14
  612.7 100.6 %copy-start.3 = (bf16[256,1024]{0,1:T(8,128)(2,1)S(1)}, bf16[256,1024]{0,1:T(8,128)(2,1)}, u32[]{:S(2)}) copy-start(bf16[256,1024]{0,1:T(8,128)(2,1)} %all_gather.78) | copy-start | bytes 1572868
Sparse Core Ops, SparseCore 0:
  10.8 63.1 all-gather.21
  76.7 59.1 all-gather.23
  138.7 54.1 all-gather.31
  195.5 53.9 all-gather.33
  252.1 59.1 all-gather.35
  313.9 59.2 all-gather.25
  376.0 59.2 all-gather.27
  438.1 74.3 all-gather.39
  515.3 74.3 all-gather.41
  592.3 58.9 all-gather.29
  654.1 59.1 all-gather.37
where the time goes:
time: 724 us; the launch traced here: 723 us
  waiting for transfers between devices  440 us (61%)
  blocking collectives  165 us (23%)
  matrix products  66.3 us (9%)
  local copies, waits for them, and re-layouts  15.5 us (2%)
  other arithmetic  15.4 us (2%)
  between operations  15.1 us (2%)
    all_gather x1, waiting for transfers between devices, gather_states(): lax.all_gather(forward_sum[1][None], 'sp', axis=0, tiled=True)  73.5 us
    all_gather x1, waiting for transfers between devices, on_device(): lax.all_gather(out_a_weight, 'sp', axis=0, tiled=True)  59.7 us
    all_gather x1, waiting for transfers between devices, on_device(): lax.all_gather(mk_weight, 'sp', axis=0, tiled=True)  59.6 us
    all_gather x1, waiting for transfers between devices, on_device(): lax.all_gather(av_weight, 'sp', axis=0, tiled=True)  54.5 us
    all_gather x1, waiting for transfers between devices, gather_states(): lax.all_gather(backward_sum[1][None], 'sp', axis=0, tiled=True)  52.6 us
    all_gather x1, waiting for transfers between devices, on_device(): lax.all_gather(aq_weight, 'sp', axis=0, tiled=True)  48.2 us
    all_gather x1, blocking collectives, on_device(): lax.all_gather(gate_weight, 'sp', axis=0, tiled=True)  43.3 us
    unnamed x1, blocking collectives  39.7 us
  transfers between devices with their start and end apart: 13, of which 13 were waited for; matrix products, arithmetic and copies ran while one was open for 13% of the time, Pallas kernels for 0%

commit v1 on v0

v1 whole, which is shorter than its diff:
```python
import functools

import jax
import jax.numpy as jnp
from jax import lax
from jax.experimental import pallas as pl
from jax.experimental.pallas import tpu as pltpu
from jax.sharding import PartitionSpec as P

M_DIM = 128
W_DIM = 64
WINDOW = 128
STATE_ROWS = 136


EPS = 1e-06
FLOOR_LOG = -1e30
HIGHEST = lax.Precision.HIGHEST
MESH = pl.DeviceIdType.MESH


def rms_rows(inputs, gain_vec):
    return inputs * lax.rsqrt(jnp.mean(inputs * inputs, axis=-1, keepdims=True) + EPS) * gain_vec


def stored(result):
    return lax.optimization_barrier(result.astype(jnp.bfloat16))


def remote(src, dst, send_sem, recv_sem, **where):
    return pltpu.make_async_remote_copy(
        src_ref=src,
        dst_ref=dst,
        send_sem=send_sem,
        recv_sem=recv_sem,
        device_id=where,
        device_id_type=MESH,
    )


def greet(peers):
    barrier = pltpu.get_barrier_semaphore()
    for peer in peers:
        pl.semaphore_signal(barrier, inc=1, device_id=peer, device_id_type=MESH)
    pl.semaphore_wait(barrier, len(peers))


def gather_kernel(
    n,
    g,
    w_ref,
    gt_ref,
    dec_ref,
    tok_ref,
    w_out,
    gt_out,
    dec_out,
    tok_out,
    own_sem,
    in_send,
    in_recv,
    tok_send,
    tok_recv,
    dec_send,
    dec_recv,
    gt_send,
    gt_recv,
    line_send,
    line_recv,
):
    me = lax.axis_index("sp")
    ng = n // g
    q = lax.div(me, g)
    h = lax.rem(me, g)
    greet([{"sp": lax.rem(me + k, n)} for k in range(1, n)])

    def row(k, d):
        return (q + k) * g + lax.rem(h - d + g, g)

    inner = []
    for d in range(1, g):
        to = lax.rem(h + d, g)
        copy = remote(
            w_ref.at[to], w_out.at[me], in_send.at[d - 1], in_recv.at[d - 1], sp=q * g + to
        )
        copy.start()
        inner.append(copy)

    def up(k, d):
        src = w_ref.at[h] if k == 0 and d == 0 else w_out.at[row(-k, d)]
        return remote(
            src,
            w_out.at[row(-k, d)],
            line_send.at[0, k, d],
            line_recv.at[0, k, d],
            sp=me + g,
        )

    def down(k, d):
        src = w_ref.at[h] if k == 0 and d == 0 else w_out.at[row(k, d)]
        return remote(
            src,
            w_out.at[row(k, d)],
            line_send.at[1, k, d],
            line_recv.at[1, k, d],
            sp=me - g,
        )

    def came_up(k, d):
        ref = w_out.at[row(-k, d)]
        return remote(ref, ref, line_send.at[0, k - 1, d], line_recv.at[0, k - 1, d], sp=me)

    def came_down(k, d):
        ref = w_out.at[row(k, d)]
        return remote(ref, ref, line_send.at[1, k - 1, d], line_recv.at[1, k - 1, d], sp=me)

    others = []
    for k in range(ng):
        for d in range(g):
            if k == 0 and d > 0:
                inner[d - 1].wait_recv()
            if k > 0:

                @pl.when(q >= k)
                def _():
                    came_up(k, d).wait_recv()

                @pl.when(q + k < ng)
                def _():
                    came_down(k, d).wait_recv()

            if k < ng - 1:

                @pl.when((q < ng - 1) & (q >= k))
                def _():
                    up(k, d).start()

                @pl.when((q > 0) & (q + k < ng))
                def _():
                    down(k, d).start()

            if k == 0 and d == 0:
                own = [
                    pltpu.make_async_copy(w_ref.at[h], w_out.at[me], own_sem.at[0]),
                    pltpu.make_async_copy(gt_ref.at[h], gt_out.at[me], own_sem.at[1]),
                    pltpu.make_async_copy(dec_ref.at[h], dec_out.at[h], own_sem.at[2]),
                    pltpu.make_async_copy(tok_ref, tok_out.at[h], own_sem.at[3]),
                ]
                for copy in own:
                    copy.start()
                for j in range(1, n):
                    peer = lax.rem(me + j, n)
                    copy = remote(
                        gt_ref.at[lax.rem(peer, g)],
                        gt_out.at[me],
                        gt_send.at[j - 1],
                        gt_recv.at[j - 1],
                        sp=peer,
                    )
                    copy.start()
                    others.append(copy)
                for j in range(1, g):
                    to = lax.rem(h + j, g)
                    copy = remote(
                        dec_ref.at[to],
                        dec_out.at[h],
                        dec_send.at[j - 1],
                        dec_recv.at[j - 1],
                        sp=q * g + to,
                    )
                    copy.start()
                    others.append(copy)
                    copy = remote(
                        tok_ref,
                        tok_out.at[h],
                        tok_send.at[j - 1],
                        tok_recv.at[j - 1],
                        sp=q * g + to,
                    )
                    copy.start()
                    others.append(copy)

    for k in range(ng - 1):
        for d in range(g):

            @pl.when((q < ng - 1) & (q >= k))
            def _():
                up(k, d).wait_send()

            @pl.when((q > 0) & (q + k < ng))
            def _():
                down(k, d).wait_send()

    for copy in inner:
        copy.wait_send()
    for copy in others:
        copy.wait()
    for copy in own:
        copy.wait()


def gather_inputs(n, g, packed, gates_t, decay, normed):
    vmem = pl.BlockSpec(memory_space=pltpu.VMEM)
    hbm = pl.BlockSpec(memory_space=pl.ANY)
    dma = pltpu.SemaphoreType.DMA
    few, ng = max(g - 1, 1), n // g
    return pl.pallas_call(
        functools.partial(gather_kernel, n, g),
        name="gather_inputs",
        out_shape=(
            jax.ShapeDtypeStruct((n,) + packed.shape[1:], packed.dtype),
            jax.ShapeDtypeStruct((n,) + gates_t.shape[1:], gates_t.dtype),
            jax.ShapeDtypeStruct(decay.shape, decay.dtype),
            jax.ShapeDtypeStruct((g,) + normed.shape, normed.dtype),
        ),
        in_specs=[vmem] * 4,
        out_specs=(hbm,) * 4,
        scratch_shapes=[
            dma((4,)),
            dma((few,)),
            dma((few,)),
            dma((few,)),
            dma((few,)),
            dma((few,)),
            dma((few,)),
            dma((n - 1,)),
            dma((n - 1,)),
            dma((2, ng, g)),
            dma((2, ng, g)),
        ],
        compiler_params=pltpu.CompilerParams(collective_id=0, has_side_effects=True),
        cost_estimate=pl.CostEstimate(
            flops=0, bytes_accessed=100_000_000, transcendentals=0
        ),
    )(packed, gates_t, decay, normed)


def state_kernel(
    ng, g, st_ref, kv_ref, st_out, kv_out, up_send, up_recv, dn_send, dn_recv, kv_send, kv_recv
):
    me = lax.axis_index("sp")
    q = lax.div(me, g)
    greet([{"sp": lax.rem(me + k * g, ng * g)} for k in range(1, ng)])
    rows = kv_ref.shape[0]

    def up(k):
        return remote(st_ref.at[0], st_out.at[q], up_send.at[k], up_recv.at[k], sp=me + k * g)

    def down(k):
        return remote(st_ref.at[1], st_out.at[q], dn_send.at[k], dn_recv.at[k], sp=me - k * g)

    def came_up(k):
        return remote(st_ref.at[0], st_out.at[q - k], up_send.at[k], up_recv.at[k], sp=me)

    def came_down(k):
        return remote(st_ref.at[1], st_out.at[q + k], dn_send.at[k], dn_recv.at[k], sp=me)

    def edge(side, peer):
        src = kv_ref.at[pl.ds(rows - WINDOW if side == 0 else 0, WINDOW)]
        return remote(src, kv_out.at[side], kv_send.at[side], kv_recv.at[side], sp=peer)

    if ng > 1:

        @pl.when(q < ng - 1)
        def _():
            edge(0, me + g).start()

        @pl.when(q > 0)
        def _():
            edge(1, me - g).start()

    for k in range(1, ng):

        @pl.when(q + k < ng)
        def _():
            up(k).start()

        @pl.when(q >= k)
        def _():
            down(k).start()

    for k in range(1, ng):

        @pl.when(q + k < ng)
        def _():
            up(k).wait_send()
            came_down(k).wait_recv()

        @pl.when(q >= k)
        def _():
            down(k).wait_send()
            came_up(k).wait_recv()

    if ng > 1:

        @pl.when(q < ng - 1)
        def _():
            edge(0, me + g).wait_send()
            edge(1, me).wait_recv()

        @pl.when(q > 0)
        def _():
            edge(1, me - g).wait_send()
            edge(0, me).wait_recv()


def exchange_states(n, g, states, kv_pairs):
    ng = n // g
    vmem = pl.BlockSpec(memory_space=pltpu.VMEM)
    dma = pltpu.SemaphoreType.DMA
    return pl.pallas_call(
        functools.partial(state_kernel, ng, g),
        name="exchange_states",
        out_shape=(
            jax.ShapeDtypeStruct((ng,) + states.shape[1:], states.dtype),
            jax.ShapeDtypeStruct((2, WINDOW, kv_pairs.shape[1]), kv_pairs.dtype),
        ),
        in_specs=[vmem] * 2,
        out_specs=(vmem,) * 2,
        scratch_shapes=[dma((ng,))] * 4 + [dma((2,))] * 2,
        compiler_params=pltpu.CompilerParams(collective_id=1, has_side_effects=True),
        cost_estimate=pl.CostEstimate(flops=0, bytes_accessed=10_000_000, transcendentals=0),
    )(states, kv_pairs)


def mix_kernel(g, tp, mx_ref, lt_ref, mx_out, lt_out, own_sem, mx_send, mx_recv, lt_send, lt_recv):
    me, c = lax.axis_index("sp"), lax.axis_index("tp")
    q, h = lax.div(me, g), lax.rem(me, g)
    total = g * tp
    mine = h * tp + c
    peers = []
    for k in range(1, total):
        to = lax.rem(mine + k, total)
        peers.append((lax.div(to, tp), lax.rem(to, tp)))
    greet([{"sp": q * g + a, "tp": b} for a, b in peers])
    copies = []
    for k, (a, b) in enumerate(peers):
        copies.append(
            remote(
                mx_ref.at[a], mx_out.at[mine], mx_send.at[k], mx_recv.at[k], sp=q * g + a, tp=b
            )
        )
    for d in range(1, g):
        a = lax.rem(h + d, g)
        copies.append(
            remote(lt_ref.at[a], lt_out.at[h], lt_send.at[d - 1], lt_recv.at[d - 1], sp=q * g + a)
        )
    own = [
        pltpu.make_async_copy(mx_ref.at[h], mx_out.at[mine], own_sem.at[0]),
        pltpu.make_async_copy(lt_ref.at[h], lt_out.at[h], own_sem.at[1]),
    ]
    for copy in copies + own:
        copy.start()
    for copy in copies + own:
        copy.wait()


def exchange_mixed(g, tp, mixed, logs):
    vmem = pl.BlockSpec(memory_space=pltpu.VMEM)
    dma = pltpu.SemaphoreType.DMA
    few, many = max(g - 1, 1), max(g * tp - 1, 1)
    return pl.pallas_call(
        functools.partial(mix_kernel, g, tp),
        name="exchange_mixed",
        out_shape=(
            jax.ShapeDtypeStruct((g * tp,) + mixed.shape[1:], mixed.dtype),
            jax.ShapeDtypeStruct(logs.shape, logs.dtype),
        ),
        in_specs=[vmem] * 2,
        out_specs=(vmem,) * 2,
        scratch_shapes=[dma((2,)), dma((many,)), dma((many,)), dma((few,)), dma((few,))],
        compiler_params=pltpu.CompilerParams(collective_id=2, has_side_effects=True),
        cost_estimate=pl.CostEstimate(flops=0, bytes_accessed=10_000_000, transcendentals=0),
    )(mixed, logs)


def window_attend(a_query, filled_margin, sink_logit, first_row, total_rows):
    tok_rows = a_query.shape[0]
    block_len = WINDOW
    block_count = tok_rows // block_len
    kv_width = filled_margin.shape[1] // 2
    kv_heads = kv_width // W_DIM
    q_heads = a_query.shape[1] // W_DIM
    groups = q_heads // kv_heads
    windows = jnp.concatenate(
        [
            filled_margin[place_idx * block_len : place_idx * block_len + tok_rows].reshape(
                block_count, block_len, 2 * kv_width
            )
            for place_idx in range(3)
        ],
        axis=1,
    )
    key_block = windows[:, :, :kv_width].reshape(block_count, 3 * block_len, kv_heads, W_DIM)
    content_tile = windows[:, :, kv_width:].reshape(block_count, 3 * block_len, kv_heads, W_DIM)
    query_block = a_query.reshape(block_count, block_len, kv_heads, groups, W_DIM)
    scores = jnp.einsum(
        "nqgrd,nkgd->ngrqk", query_block, key_block, preferred_element_type=jnp.float32
    ) * W_DIM ** (-0.5)
    query_off = jnp.arange(block_len, dtype=jnp.int32)
    key_off = jnp.arange(3 * block_len, dtype=jnp.int32) - block_len
    in_window = jnp.abs(query_off[:, None] - key_off[None, :]) <= WINDOW
    key_place = (
        first_row + jnp.arange(block_count, dtype=jnp.int32)[:, None] * block_len + key_off[None, :]
    )
    inside = (key_place >= 0) & (key_place < total_rows)
    usable = in_window[None] & inside[:, None, :]
    scores = jnp.where(usable[:, None, None], scores, -jnp.inf)
    sink_col = sink_logit.reshape(kv_heads, groups)[None, :, :, None]
    peak_log = jnp.maximum(sink_col, jnp.max(scores, axis=-1))
    weights_exp = jnp.exp(scores - peak_log[..., None])
    weight_total_sum = jnp.exp(sink_col - peak_log) + jnp.sum(weights_exp, axis=-1)
    weighted = jnp.einsum(
        "ngrqk,nkgd->nqgrd",
        weights_exp.astype(jnp.bfloat16),
        content_tile,
        preferred_element_type=jnp.float32,
    )
    scale_back = jnp.transpose(weight_total_sum, (0, 3, 1, 2))[..., None]
    mixed_rows = (weighted / scale_back).astype(jnp.bfloat16).reshape(tok_rows, q_heads * W_DIM)
    log_total = jnp.transpose(peak_log + jnp.log(weight_total_sum), (1, 2, 0, 3)).reshape(
        q_heads, tok_rows
    )
    return (mixed_rows, log_total)


def on_device(
    tokens,
    input_norm_gain,
    mq_weight,
    mk_weight,
    mv_weight,
    mo_weight,
    gate_weight,
    gate_bias,
    decay_extra,
    m_gain,
    aq_weight,
    ak_weight,
    av_weight,
    sink_logit,
    out_m_weight,
    out_a_weight,
):
    n, tp = lax.axis_size("sp"), lax.axis_size("tp")
    tok_rows = tokens.shape[0]
    local_heads = gate_weight.shape[2]
    g = 1
    while local_heads % (2 * g) == 0 and n % (2 * g) == 0 and ak_weight.shape[1] % (2 * g * W_DIM) == 0:
        g *= 2
    ng, heads = n // g, local_heads // g
    own = lax.axis_index("sp")
    q, h = lax.div(own, g), lax.rem(own, g)
    rows = mq_weight.shape[0]
    length = g * tok_rows

    normed = rms_rows(tokens.astype(jnp.float32), input_norm_gain).astype(jnp.bfloat16)
    weights = (mq_weight, mk_weight, mv_weight, mo_weight, aq_weight, ak_weight, av_weight)
    packed = jnp.concatenate([w.reshape(rows, g, -1) for w in weights], axis=2)
    packed = jnp.transpose(packed, (1, 0, 2))
    gates_t = jnp.transpose(gate_weight.reshape(rows, 4, g, heads), (2, 1, 3, 0))
    gates_t = gates_t.reshape(g, 4 * heads, rows)
    gates_t = jnp.pad(gates_t, ((0, 0), (0, -(4 * heads) % 16), (0, 0)))
    decay = jnp.transpose(decay_extra.reshape(2, g, heads, tok_rows), (1, 0, 2, 3))
    decay = decay.reshape(g, 2 * heads, tok_rows)
    decay = jnp.pad(decay, ((0, 0), (0, -(2 * heads) % 8), (0, 0)))

    out_w = jnp.concatenate([out_m_weight, out_a_weight], axis=0)
    out_w = lax.all_gather(out_w, "sp", axis=0, tiled=True)

    w_all, gt_all, dec_all, tok_all = gather_inputs(n, g, packed, gates_t, decay, normed)
    tok_all = tok_all.reshape(length, -1)
    w_all = w_all.reshape(n * rows, -1)
    widths = [w.shape[1] // g for w in weights]
    starts = [sum(widths[:i]) for i in range(len(widths) + 1)]
    projected = stored(jnp.dot(tok_all, w_all, preferred_element_type=jnp.float32))
    m_query, m_key, m_value, m_out, a_query, a_key, a_value = [
        projected[:, a:b] for a, b in zip(starts[:-1], starts[1:])
    ]
    kv_pairs = projected[:, starts[5] :]
    gt_rows = jnp.transpose(gt_all, (0, 2, 1)).reshape(n * rows, -1)
    gates = jnp.dot(tok_all, gt_rows, preferred_element_type=jnp.float32)
    gates = gates[:, : 4 * heads].T.reshape(4, heads, length)
    gates = gates + lax.dynamic_slice_in_dim(gate_bias, h * heads, heads, 1)[:, :, None]
    gates = gates.reshape(4, heads, g, tok_rows)
    decay = jnp.transpose(dec_all[:, : 2 * heads], (1, 0, 2)).reshape(2, heads, g, tok_rows)
    in_gate = jnp.stack([gates[0], gates[2]])
    forget = jax.nn.log_sigmoid(jnp.stack([gates[1], gates[3]])) + decay

    def chunks(matrix):
        return jnp.transpose(matrix.reshape(g, tok_rows, heads, M_DIM), (2, 0, 1, 3))

    queries, keys, values = chunks(m_query), chunks(m_key), chunks(m_value)
    queries32, values32 = queries.astype(jnp.float32), values.astype(jnp.float32)
    keys32 = keys.astype(jnp.float32) * M_DIM ** (-0.5)

    place = jnp.arange(tok_rows, dtype=jnp.int32)
    before = place[:, None] <= place[None, :]
    reach = jnp.stack([before, before.T])
    cum = jnp.einsum("dhcs,dst->dhct", forget, reach.astype(jnp.float32), precision=HIGHEST)
    total = jnp.sum(forget, axis=-1)
    log_end = total[..., None] - cum + in_gate
    peak = jnp.max(log_end, axis=-1)
    w_end = jnp.exp(log_end - peak[..., None])
    faded = w_end[..., None] * keys32[None]
    cells = jnp.einsum("dhcsk,hcsv->dhckv", faded, values32, precision=HIGHEST)
    norms = jnp.sum(faded, axis=3)
    summary = jnp.concatenate([cells, norms[..., None, :]], axis=3)

    at = jnp.arange(g, dtype=jnp.int32)
    later = at[:, None] < at[None, :]
    c_, j_, i_ = at[:, None, None], at[None, :, None], at[None, None, :]
    between = jnp.stack([(j_ < i_) & (i_ < c_), (c_ < i_) & (i_ < j_)]).astype(jnp.float32)
    log_local = peak[:, :, None, :] + jnp.einsum(
        "dcji,dhi->dhcj", between, total, precision=HIGHEST
    )
    local_ok = jnp.stack([later.T, later])[:, None]
    to_end = jnp.stack([later, later.T]).astype(jnp.float32)
    log_group = peak + jnp.einsum("dji,dhi->dhj", to_end, total, precision=HIGHEST)
    group_peak = jnp.max(log_group, axis=-1)
    group_scale = jnp.exp(log_group - group_peak[..., None])
    group_sum = jnp.sum(group_scale[..., None, None] * summary, axis=2)
    group_total = jnp.sum(total, axis=-1)
    logs = jnp.stack([group_peak, group_total], axis=-1)[..., None]
    logs = jnp.broadcast_to(logs, logs.shape[:-1] + (M_DIM,))
    message = jnp.concatenate([group_sum, logs], axis=2)
    message = jnp.pad(message, ((0, 0), (0, 0), (0, STATE_ROWS - message.shape[2]), (0, 0)))
    message = message.reshape(2, heads * STATE_ROWS, M_DIM)

    came, edges = exchange_states(n, g, message, kv_pairs)
    came = came.reshape(ng, heads, STATE_ROWS, M_DIM)
    who = jnp.arange(ng, dtype=jnp.int32)
    came = jnp.where((who != q)[:, None, None, None], came, 0.0)
    outer_sum = came[:, :, : M_DIM + 1]
    outer_peak, outer_total = came[:, :, M_DIM + 1, 0], came[:, :, M_DIM + 2, 0]
    o_, u_ = who[:, None], who[None, :]
    crossed = ((o_ < u_) & (u_ < q)) | ((q < u_) & (u_ < o_))
    log_outer = outer_peak + jnp.einsum(
        "ou,uh->oh", crossed.astype(jnp.float32), outer_total, precision=HIGHEST
    )
    lead = jnp.einsum(
        "dci,dhi->dhc", jnp.stack([later.T, later]).astype(jnp.float32), total, precision=HIGHEST
    )
    log_outer = log_outer.T[None, :, None, :] + lead[..., None]
    outer_ok = jnp.stack([who < q, who > q])[:, None, None, :]
    log_src = jnp.concatenate(
        [
            jnp.where(local_ok, log_local, FLOOR_LOG),
            jnp.where(outer_ok, log_outer, FLOOR_LOG),
        ],
        axis=-1,
    )
    ok = jnp.concatenate(
        [jnp.broadcast_to(local_ok, log_local.shape), jnp.broadcast_to(outer_ok, log_outer.shape)],
        axis=-1,
    )
    in_peak = jnp.max(log_src, axis=-1)
    scale = jnp.where(ok, jnp.exp(log_src - in_peak[..., None]), 0.0)
    state = jnp.sum(scale[..., :g, None, None] * summary[:, :, None], axis=3)
    for o in range(ng):
        state = state + scale[..., g + o, None, None] * outer_sum[o][None, :, None]

    log_w = jnp.where(
        jnp.swapaxes(reach, 1, 2)[:, None, None],
        cum[..., :, None] - cum[..., None, :] + in_gate[..., None, :],
        -jnp.inf,
    )
    log_inter = cum + in_peak[..., None]
    row_max = jnp.maximum(jnp.maximum(log_inter, jnp.max(log_w, axis=-1)), 0.0)
    w_inter = jnp.exp(log_inter - row_max)
    scores = jnp.einsum("hctk,hcsk->hcts", queries, keys, preferred_element_type=jnp.float32)
    scores = (scores * M_DIM ** (-0.5))[None] * jnp.exp(log_w - row_max[..., None])
    numer = jnp.einsum("dhcts,hcsv->dhctv", scores, values32, precision=HIGHEST)
    numer = numer + w_inter[..., None] * jnp.einsum(
        "hctk,dhckv->dhctv", queries32, state[..., :M_DIM, :], precision=HIGHEST
    )
    denom = jnp.sum(scores, axis=-1) + w_inter * jnp.sum(
        queries32[None] * state[..., M_DIM:, :], axis=-1
    )
    parts = numer / jnp.maximum(jnp.abs(denom), jnp.exp(-row_max))[..., None]
    cell_rows = jnp.transpose(parts[0] + parts[1], (1, 2, 0, 3)).reshape(length, heads, M_DIM)
    gate_open = jax.nn.sigmoid(m_out.astype(jnp.float32)).reshape(length, heads, M_DIM)
    gain = lax.dynamic_slice_in_dim(m_gain, h * heads * M_DIM, heads * M_DIM, 0)
    mixed_m = (
        rms_rows(cell_rows * gate_open, gain.reshape(heads, M_DIM))
        .astype(jnp.bfloat16)
        .reshape(length, heads * M_DIM)
    )

    edge_ok = jnp.stack([q > 0, q < ng - 1])[:, None, None]
    edges = jnp.where(edge_ok, edges, jnp.zeros_like(edges))
    margin = jnp.concatenate([edges[0], kv_pairs, edges[1]], axis=0)
    sinks = sink_logit.shape[0] // g
    sink = lax.dynamic_slice_in_dim(sink_logit, h * sinks, sinks, 0)
    mixed_a, log_total = window_attend(a_query, margin, sink, q * length, n * tok_rows)

    both = jnp.concatenate([mixed_m, mixed_a], axis=1).reshape(g, tok_rows, -1)
    logs = jnp.transpose(log_total.reshape(sinks, g, tok_rows), (1, 0, 2))
    logs = jnp.pad(logs, ((0, 0), (0, -sinks % 8), (0, 0)))
    mixed_all, logs_all = exchange_mixed(g, tp, both, logs)
    log_total = logs_all[:, :sinks].reshape(g * sinks, tok_rows)
    mixed_all = mixed_all.reshape(g, tp, tok_rows, -1)
    mixed_all = jnp.transpose(mixed_all, (2, 1, 0, 3))
    m_cols = mixed_m.shape[1]
    full_m = mixed_all[..., :m_cols].reshape(tok_rows, n, -1)
    full_a = mixed_all[..., m_cols:].reshape(tok_rows, n, -1)
    full = jnp.concatenate([full_m, full_a], axis=2).reshape(tok_rows, -1)
    mixed = jnp.dot(full, out_w, preferred_element_type=jnp.float32)
    return (mixed.astype(jnp.bfloat16), log_total)


def solution(mesh):
    in_specs = (
        P("sp", None),
        P(),
        P("sp", "tp"),
        P("sp", "tp"),
        P("sp", "tp"),
        P("sp", "tp"),
        P("sp", None, "tp"),
        P(None, "tp"),
        P(None, "tp", "sp"),
        P("tp"),
        P("sp", "tp"),
        P("sp", "tp"),
        P("sp", "tp"),
        P("tp"),
        P("sp", "tp"),
        P("sp", "tp"),
    )
    out_specs = (P("sp", "tp"), P("tp", "sp"))
    return jax.shard_map(
        on_device, mesh=mesh, in_specs=in_specs, out_specs=out_specs, check_vma=False
    )
```

time: 724 us -> 208 us (0.29)
  waiting for transfers between devices: 440 us -> 0.04 us
  blocking collectives: 165 us -> 0 us
  Pallas kernels: 0 us -> 128 us
  matrix products: 66.3 us -> 20.9 us
  local copies, waits for them, and re-layouts: 15.5 us -> 23.6 us
    all_gather x11 -> x1, waiting for transfers between devices: 429 us -> 0.02 us  [on_device(): out_w = lax.all_gather(out_w, 'sp', axis=0, tiled=True)]
    pallas_call x0 -> x3, Pallas kernels: none -> 128 us  [the longest x1 99.8 us: gather_inputs(): pl.pallas_call(functools.partial(gather_kernel, n, g), name='gather_input...]
    all_gather x5 -> x0, blocking collectives: 126 us -> none  [the longest x1 43.3 us: on_device(): lax.all_gather(gate_weight, 'sp', axis=0, tiled=True)]
    dot_general x66 -> x12, matrix products: 64.7 us -> 19.2 us  [the longest x1 6.57 us: on_device(): jnp.dot(tok_all, w_all, preferred_element_type=jnp.float32)]
    unnamed x1 -> x0, blocking collectives: 39.7 us -> none
  transfers between devices with their start and end apart: 13 -> 1, of which waited for: 13 -> 0; matrix products, arithmetic and copies ran while one was open for 13% -> 28% of each run, Pallas kernels for 0% -> 62%
where the time goes in v1:
time: 208 us; the launch traced here: 207 us
  Pallas kernels  128 us (62%)
  local copies, waits for them, and re-layouts  23.6 us (11%)
  matrix products  20.9 us (10%)
  other arithmetic  19.9 us (10%)
  between operations  14.8 us (7%)
    pallas_call x1, Pallas kernels, gather_inputs(): pl.pallas_call(functools.partial(gather_kernel, n, g), name='gather_input...  99.8 us
    pallas_call x1, Pallas kernels, exchange_mixed(): pl.pallas_call(functools.partial(mix_kernel, g, tp), name='exchange_mixed...  18 us
    pallas_call x1, Pallas kernels, exchange_states(): pl.pallas_call(functools.partial(state_kernel, ng, g), name='exchange_sta...  9.98 us
    dot_general x1, matrix products, on_device(): jnp.dot(tok_all, w_all, preferred_element_type=jnp.float32)  6.57 us
    mul x9, local copies, waits for them, and re-layouts, on_device(): state = state + scale[..., g + o, None, None] * outer_sum[o][None, :, None]  5.12 us
    dot_general x1, matrix products, on_device(): mixed = jnp.dot(full, out_w, preferred_element_type=jnp.float32)  4.25 us
  transfers between devices with their start and end apart: 1, of which 0 were waited for; matrix products, arithmetic and copies ran while one was open for 28% of the time, Pallas kernels for 62%

profile of v1, /device:TPU:0, one launch (start us, length us, event | category | flops | bytes accessed | tf_op | source)
XLA Modules:
  0.0 207.0 jit_solution(18256885165766188224)
XLA Ops:
  7.3 1.8 pad_maximum_fusion.6
  9.2 1.0 copy.211
  10.4 1.0 copy.212
  11.6 1.0 copy.213
  14.2 1.3 fusion.5.tok_ref
  15.5 0.6 pad.16.dec_ref
  16.1 0.6 pad.15.gt_ref
  16.7 1.1 concatenate.73
  17.8 99.8 %gather_inputs.1 = (bf16[16,128,768]{2,1,0:T(8,128)(2,1)}, bf16[16,16,128]{2,1,0:T(8,128)(2,1)}, f32[4,8,256]{2,1,0:T(8,128)}, bf16[4,256,2048]{2,1,0:T(8,128)(2,1)}) custom-call(bf16[4,128,768]{2,1,0:T(8,128)(2,1)} %bitcast.247, bf16[4,16,128]{2,1,0:T(8,128)(2,1)} %pad.15.gt_ref, f32[4,8,256]{2,1,0:T(8,128)} %pad.16.dec_ref, bf16[256,2048]{1,0:T(8,128)(2,1)} %fusion.5.tok_ref), custom_call_target="tpu_custom_call" | custom-call | bytes 100000000 | tf_op jit(solution)/shard_map/gather_inputs/pallas_call | solution.py:207
  117.7 0.8 copy_bitcast_fusion
  118.7 3.4 %fusion.27 = f32[4,1024]{1,0:T(4,128)S(1)} fusion(bf16[1024,2048]{1,0:T(8,128)(2,1)} %bitcast.243, bf16[2048,16]{0,1:T(8,128)(2,1)S(1)} %copy_bitcast_fusion, f32[4]{0:T(128)S(1)} %dynamic-slice_reduce_fusion), kind=kOutput, calls=%fused_computation.35 | convolution fusion | flops 16781312 | bytes 4227584 | tf_op jit(solution)/shard_map/dot_general | solution.py:482
  122.1 0.6 slice_reduce_fusion.3
  122.7 1.0 fusion.80
  124.2 6.6 %convolution_convert_fusion = bf16[1024,768]{1,0:T(8,128)(2,1)S(1)} fusion(bf16[1024,2048]{1,0:T(8,128)(2,1)} %bitcast.244, bf16[2048,768]{1,0:T(8,128)(2,1)} %bitcast.293), kind=kOutput, calls=%fused_computation.21 | convolution fusion | flops 3222011904 | bytes 8912896 | tf_op jit(solution)/shard_map/dot_general | solution.py:476
  130.8 1.3 bitcast_convert_fusion
  133.4 0.6 convolution_bitcast_fusion.1
  134.3 0.7 fusion.53.st_ref
  134.9 10.0 %exchange_states.1 = (f32[4,136,128]{2,1,0:T(8,128)}, bf16[2,128,128]{2,1,0:T(8,128)(2,1)}) custom-call(f32[2,136,128]{2,1,0:T(8,128)} %fusion.53.st_ref, bf16[1024,128]{1,0:T(8,128)(2,1)} %get-tuple-element.33.kv_ref), custom_call_target="tpu_custom_call" | custom-call | bytes 10000000 | tf_op jit(solution)/shard_map/exchange_states/pallas_call | solution.py:311
  144.9 1.0 select_bitcast_fusion
  147.1 0.6 copy.230
  148.0 1.3 multiply_reduce_fusion
  149.8 0.7 copy.281
  150.5 0.7 copy.282
  151.2 0.7 copy.283
  151.9 0.7 copy.284
  152.7 0.8 copy.249
  153.4 0.8 copy.251
  154.2 0.8 copy.253
  154.9 1.4 fusion.31
  156.6 0.7 slice.135
  157.3 0.9 fusion.52
  158.5 0.7 fusion.10
  160.0 1.1 multiply_reduce_fusion.1
  161.1 2.4 %fusion.18 = f32[2,1,4,256,128]{3,4,0,2,1:T(8,128)S(1)} fusion(bf16[4,256,128,1]{2,1,3,0:T(8,128)(2,1)S(1)} %bitcast.253, f32[2,4,256]{2,0,1:T(2,128)S(1)} %get-tuple-element.25, f32[2,4,256]{2,0,1:T(2,128)S(1)} %copy.232, f32[2,4,256]{2,0,1:T(2,128)S(1)} %copy-done.16, f32[4,256,256]{2,1,0:T(8,128)S(1)} %convolution_multiply_fusion, ...), kind=kOutput, calls=%fused_computation.25 | convolution fusion | flops 807927808 | bytes 2514944 | tf_op jit(solution)/shard_map/dhcts,hcsv->dhctv/dot_general | solution.py:573
  163.5 0.6 fusion.23
  167.1 0.7 fusion.2
  167.9 0.7 fusion
  168.7 0.9 fusion.43
  170.3 0.6 pad.18.lt_ref
  170.9 0.8 dynamic_slice.10
  171.6 1.2 multiply_reduce_fusion.5
  172.8 1.2 multiply_convert_fusion
  174.0 0.9 pad_maximum_fusion.3.mx_ref
  174.8 18.0 %exchange_mixed.1 = (bf16[8,256,256]{2,1,0:T(8,128)(2,1)}, f32[4,8,256]{2,1,0:T(8,128)}) custom-call(bf16[4,256,256]{2,1,0:T(8,128)(2,1)} %pad_maximum_fusion.3.mx_ref, f32[4,8,256]{2,1,0:T(8,128)} %pad.18.lt_ref), custom_call_target="tpu_custom_call" | custom-call | bytes 10000000 | tf_op jit(solution)/shard_map/exchange_mixed/pallas_call | solution.py:362
  192.8 1.5 copy.267
  194.3 0.8 slice.164
  195.1 0.6 reshape.871
  195.9 4.3 %convolution_convert_fusion.1 = bf16[256,1024]{1,0:T(8,128)(2,1)} fusion(bf16[256,2048]{0,1:T(8,128)(2,1)S(1)} %bitcast.254, bf16[2048,1024]{1,0:T(8,128)(2,1)} %all-gather.2.cloned.1.call-done), kind=kOutput, calls=%fused_computation.31 | convolution fusion | flops 1074003968 | bytes 5767168 | tf_op jit(solution)/shard_map/dot_general | solution.py:608
  (138 shorter events, 11.0 us)
Async XLA Ops:
  7.2 111.4 %copy-start = (f32[4,4]{1,0:T(4,128)S(1)}, f32[4,4]{1,0:T(4,128)}, u32[]{:S(2)}) copy-start(f32[4,4]{1,0:T(4,128)} %param.23) | copy-start | bytes 196
  7.2 5.6 %copy-start.7 = (bf16[128,512]{1,0:T(8,128)(2,1)S(1)}, bf16[128,512]{1,0:T(8,128)(2,1)}, u32[]{:S(2)}) copy-start(bf16[128,512]{1,0:T(8,128)(2,1)} %param.21) | copy-start | bytes 393220
  7.2 5.9 %copy-start.8 = (bf16[128,512]{1,0:T(8,128)(2,1)S(1)}, bf16[128,512]{1,0:T(8,128)(2,1)}, u32[]{:S(2)}) copy-start(bf16[128,512]{1,0:T(8,128)(2,1)} %param.26) | copy-start | bytes 393220
  7.2 6.1 %copy-start.9 = (bf16[128,256]{1,0:T(8,128)(2,1)S(1)}, bf16[128,256]{1,0:T(8,128)(2,1)}, u32[]{:S(2)}) copy-start(bf16[128,256]{1,0:T(8,128)(2,1)} %param.27) | copy-start | bytes 196612
  7.2 6.4 %copy-start.10 = (bf16[128,256]{1,0:T(8,128)(2,1)S(1)}, bf16[128,256]{1,0:T(8,128)(2,1)}, u32[]{:S(2)}) copy-start(bf16[128,256]{1,0:T(8,128)(2,1)} %param.28) | copy-start | bytes 196612
  7.2 6.6 %copy-start.2 = (bf16[256,2048]{1,0:T(8,128)(2,1)S(1)}, bf16[256,2048]{1,0:T(8,128)(2,1)}, u32[]{:S(2)}) copy-start(bf16[256,2048]{1,0:T(8,128)(2,1)} %param.16) | copy-start | bytes 3145732
  7.2 188.6 %all-gather.2.cloned.1.call-start = ((), (), s32[]{:S(2)}) async-start(), calls=%async_computation | async-start | bytes 4456448 | tf_op jit(solution)/shard_map/all_gather | solution.py:469
  9.2 114.6 %copy-start.5 = (pred[1,256,256]{2,1,0:T(32,128)(4,1)}, pred[1,256,256]{2,1,0:T(32,128)(4,1)S(1)}, u32[]{:S(2)}) copy-start(pred[1,256,256]{2,1,0:T(32,128)(4,1)S(1)} %get-tuple-element.69) | copy-start | bytes 196612
  9.2 114.6 %copy-start.6 = (pred[1,256,256]{2,1,0:T(32,128)(4,1)}, pred[1,256,256]{2,1,0:T(32,128)(4,1)S(1)}, u32[]{:S(2)}) copy-start(pred[1,256,256]{2,1,0:T(32,128)(4,1)S(1)} %get-tuple-element.70) | copy-start | bytes 196612
  10.3 3.9 %copy-start.15 = (f32[2,4,256]{2,1,0:T(4,128)S(1)}, f32[2,4,256]{2,1,0:T(4,128)}, u32[]{:S(2)}) copy-start(f32[2,4,256]{2,1,0:T(4,128)} %param.24) | copy-start | bytes 24580
  10.3 3.9 %copy-start.17 = (bf16[128,4,4]{0,2,1:T(4,128)(2,1)S(1)}, bf16[128,4,4]{0,2,1:T(4,128)(2,1)}, u32[]{:S(2)}) copy-start(bf16[128,4,4]{0,2,1:T(4,128)(2,1)} %param.22) | copy-start | bytes 12292
  10.3 3.9 %copy-start.14 = (f32[2048]{0:T(1024)S(1)}, f32[2048]{0:T(1024)}, u32[]{:S(2)}) copy-start(f32[2048]{0:T(1024)} %param.17) | copy-start | bytes 24580
  130.8 1.3 copy-start.3
  147.7 1.7 copy-start.12
  156.4 2.8 %copy-start.13 = (f32[2,4]{1,0:T(2,128)S(1)}, f32[2,4]{1,0:T(2,128)}, u32[]{:S(2)}) copy-start(f32[2,4]{1,0:T(2,128)} %copy-done.12) | copy-start | bytes 100
  156.4 3.3 %copy-start.4 = (bf16[1024,128]{1,0:T(8,128)(2,1)S(1)}, bf16[1024,128]{1,0:T(8,128)(2,1)}, u32[]{:S(2)}) copy-start(bf16[1024,128]{1,0:T(8,128)(2,1)} %get-tuple-element.35) | copy-start | bytes 786436
  156.6 4.5 %copy-start.16 = (f32[2,4,256]{2,0,1:T(2,128)S(1)}, f32[2,4,256]{2,0,1:T(2,128)}, u32[]{:S(2)}) copy-start(f32[2,4,256]{2,0,1:T(2,128)} %copy.230) | copy-start | bytes 24580
  164.2 0.8 copy-start.11
  164.2 1.0 copy-start.1
  164.3 1.8 copy-start.18
Sparse Core Ops, SparseCore 0:
  10.8 106.4 all-gather.1

commit v2 on v1

--- a/solution.py
+++ b/solution.py
@@ -52,10 +52,12 @@
     gt_ref,
     dec_ref,
     tok_ref,
+    ow_ref,
     w_out,
     gt_out,
     dec_out,
     tok_out,
+    ow_out,
     own_sem,
     in_send,
     in_recv,
@@ -67,6 +69,8 @@
     gt_recv,
     line_send,
     line_recv,
+    ow_send,
+    ow_recv,
 ):
     me = lax.axis_index("sp")
     ng = n // g
@@ -114,6 +118,22 @@
         ref = w_out.at[row(k, d)]
         return remote(ref, ref, line_send.at[1, k - 1, d], line_recv.at[1, k - 1, d], sp=me)
 
+    def out_up(k):
+        src = ow_ref if k == 0 else ow_out.at[q - k]
+        return remote(src, ow_out.at[q - k], ow_send.at[0, k], ow_recv.at[0, k], sp=me + g)
+
+    def out_down(k):
+        src = ow_ref if k == 0 else ow_out.at[q + k]
+        return remote(src, ow_out.at[q + k], ow_send.at[1, k], ow_recv.at[1, k], sp=me - g)
+
+    def out_came_up(k):
+        ref = ow_out.at[q - k]
+        return remote(ref, ref, ow_send.at[0, k - 1], ow_recv.at[0, k - 1], sp=me)
+
+    def out_came_down(k):
+        ref = ow_out.at[q + k]
+        return remote(ref, ref, ow_send.at[1, k - 1], ow_recv.at[1, k - 1], sp=me)
+
     others = []
     for k in range(ng):
         for d in range(g):
@@ -139,12 +159,34 @@
                 def _():
                     down(k, d).start()
 
+            if d == g - 1:
+                if k > 0:
+
+                    @pl.when(q >= k)
+                    def _():
+                        out_came_up(k).wait_recv()
+
+                    @pl.when(q + k < ng)
+                    def _():
+                        out_came_down(k).wait_recv()
+
+                if k < ng - 1:
+
+                    @pl.when((q < ng - 1) & (q >= k))
+                    def _():
+                        out_up(k).start()
+
+                    @pl.when((q > 0) & (q + k < ng))
+                    def _():
+                        out_down(k).start()
+
             if k == 0 and d == 0:
                 own = [
                     pltpu.make_async_copy(w_ref.at[h], w_out.at[me], own_sem.at[0]),
                     pltpu.make_async_copy(gt_ref.at[h], gt_out.at[me], own_sem.at[1]),
                     pltpu.make_async_copy(dec_ref.at[h], dec_out.at[h], own_sem.at[2]),
                     pltpu.make_async_copy(tok_ref, tok_out.at[h], own_sem.at[3]),
+                    pltpu.make_async_copy(ow_ref, ow_out.at[q], own_sem.at[4]),
                 ]
                 for copy in own:
                     copy.start()
@@ -191,6 +233,14 @@
             def _():
                 down(k, d).wait_send()
 
+        @pl.when((q < ng - 1) & (q >= k))
+        def _():
+            out_up(k).wait_send()
+
+        @pl.when((q > 0) & (q + k < ng))
+        def _():
+            out_down(k).wait_send()
+
     for copy in inner:
         copy.wait_send()
     for copy in others:
@@ -199,7 +249,7 @@
         copy.wait()
 
 
-def gather_inputs(n, g, packed, gates_t, decay, normed):
+def gather_inputs(n, g, packed, gates_t, decay, normed, out_w):
     vmem = pl.BlockSpec(memory_space=pltpu.VMEM)
     hbm = pl.BlockSpec(memory_space=pl.ANY)
     dma = pltpu.SemaphoreType.DMA
@@ -212,11 +262,12 @@
             jax.ShapeDtypeStruct((n,) + gates_t.shape[1:], gates_t.dtype),
             jax.ShapeDtypeStruct(decay.shape, decay.dtype),
             jax.ShapeDtypeStruct((g,) + normed.shape, normed.dtype),
+            jax.ShapeDtypeStruct((ng,) + out_w.shape, out_w.dtype),
         ),
-        in_specs=[vmem] * 4,
-        out_specs=(hbm,) * 4,
+        in_specs=[vmem] * 5,
+        out_specs=(hbm,) * 5,
         scratch_shapes=[
-            dma((4,)),
+            dma((5,)),
             dma((few,)),
             dma((few,)),
             dma((few,)),
@@ -227,12 +278,14 @@
             dma((n - 1,)),
             dma((2, ng, g)),
             dma((2, ng, g)),
+            dma((2, ng)),
+            dma((2, ng)),
         ],
         compiler_params=pltpu.CompilerParams(collective_id=0, has_side_effects=True),
         cost_estimate=pl.CostEstimate(
             flops=0, bytes_accessed=100_000_000, transcendentals=0
         ),
-    )(packed, gates_t, decay, normed)
+    )(packed, gates_t, decay, normed, out_w)
 
 
 def state_kernel(
@@ -456,8 +509,14 @@
 
     normed = rms_rows(tokens.astype(jnp.float32), input_norm_gain).astype(jnp.bfloat16)
     weights = (mq_weight, mk_weight, mv_weight, mo_weight, aq_weight, ak_weight, av_weight)
-    packed = jnp.concatenate([w.reshape(rows, g, -1) for w in weights], axis=2)
-    packed = jnp.transpose(packed, (1, 0, 2))
+    packed = jnp.stack(
+        [
+            jnp.concatenate(
+                [w[:, j * (w.shape[1] // g) : (j + 1) * (w.shape[1] // g)] for w in weights], axis=1
+            )
+            for j in range(g)
+        ]
+    )
     gates_t = jnp.transpose(gate_weight.reshape(rows, 4, g, heads), (2, 1, 3, 0))
     gates_t = gates_t.reshape(g, 4 * heads, rows)
     gates_t = jnp.pad(gates_t, ((0, 0), (0, -(4 * heads) % 16), (0, 0)))
@@ -466,9 +525,21 @@
     decay = jnp.pad(decay, ((0, 0), (0, -(2 * heads) % 8), (0, 0)))
 
     out_w = jnp.concatenate([out_m_weight, out_a_weight], axis=0)
-    out_w = lax.all_gather(out_w, "sp", axis=0, tiled=True)
-
-    w_all, gt_all, dec_all, tok_all = gather_inputs(n, g, packed, gates_t, decay, normed)
+    out_w_rows = out_w.shape[0]
+
+    w_all, gt_all, dec_all, tok_all, out_w = gather_inputs(
+        n, g, packed, gates_t, decay, normed, out_w
+    )
+    if g > 1:
+        planes = [[i * g + j for j in range(g)] for i in range(ng)]
+        out_w = lax.all_gather(
+            out_w.reshape(-1, out_w.shape[2]),
+            "sp",
+            axis=0,
+            axis_index_groups=planes,
+            tiled=True,
+        )
+    out_w = out_w.reshape(n * out_w_rows, -1)
     tok_all = tok_all.reshape(length, -1)
     w_all = w_all.reshape(n * rows, -1)
     widths = [w.shape[1] // g for w in weights]
@@ -604,7 +675,8 @@
     m_cols = mixed_m.shape[1]
     full_m = mixed_all[..., :m_cols].reshape(tok_rows, n, -1)
     full_a = mixed_all[..., m_cols:].reshape(tok_rows, n, -1)
-    full = jnp.concatenate([full_m, full_a], axis=2).reshape(tok_rows, -1)
+    full = jnp.concatenate([full_m, full_a], axis=2).reshape(tok_rows, ng, g, -1)
+    full = jnp.swapaxes(full, 1, 2).reshape(tok_rows, -1)
     mixed = jnp.dot(full, out_w, preferred_element_type=jnp.float32)
     return (mixed.astype(jnp.bfloat16), log_total)
 

time: 208 us -> 194 us (0.933)
  Pallas kernels: 128 us -> 111 us
  other arithmetic: 19.9 us -> 22.1 us
    pallas_call x1, Pallas kernels: 99.8 us -> 81.5 us  [gather_inputs(): pl.pallas_call(functools.partial(gather_kernel, n, g), name='gather_input...]
    slice x0 -> x4, local copies, waits for them, and re-layouts: none -> 2.81 us  [on_device(): w[:, j * (w.shape[1] // g):(j + 1) * (w.shape[1] // g)]]
    unnamed x47 -> x32, local copies, waits for them, and re-layouts: 4.16 us -> 2.02 us
  transfers between devices with their start and end apart: 1 -> 1, of which waited for: 0 -> 0; matrix products, arithmetic and copies ran while one was open for 28% -> 27% of each run, Pallas kernels for 62% -> 15%
where the time goes in v2:
time: 194 us; the launch traced here: 193 us
  Pallas kernels  111 us (57%)
  local copies, waits for them, and re-layouts  24.1 us (12%)
  other arithmetic  22.1 us (11%)
  matrix products  21.2 us (11%)
  between operations  14.7 us (8%)
    pallas_call x1, Pallas kernels, gather_inputs(): pl.pallas_call(functools.partial(gather_kernel, n, g), name='gather_input...  81.5 us
    pallas_call x1, Pallas kernels, exchange_mixed(): pl.pallas_call(functools.partial(mix_kernel, g, tp), name='exchange_mixed...  17.8 us
    pallas_call x1, Pallas kernels, exchange_states(): pl.pallas_call(functools.partial(state_kernel, ng, g), name='exchange_sta...  11.5 us
    dot_general x1, matrix products, on_device(): jnp.dot(tok_all, w_all, preferred_element_type=jnp.float32)  6.87 us
    mul x9, local copies, waits for them, and re-layouts, on_device(): state = state + scale[..., g + o, None, None] * outer_sum[o][None, :, None]  5.76 us
    dot_general x1, matrix products, on_device(): mixed = jnp.dot(full, out_w, preferred_element_type=jnp.float32)  4.25 us
  transfers between devices with their start and end apart: 1, of which 0 were waited for; matrix products, arithmetic and copies ran while one was open for 27% of the time, Pallas kernels for 15%

profile of v2, /device:TPU:0, one launch (start us, length us, event | category | flops | bytes accessed | tf_op | source)
XLA Modules:
  0.0 193.0 jit_solution(18054156126011632656)
XLA Ops:
  7.3 0.9 fusion.89
  8.2 1.5 fusion.3
  9.7 0.8 copy.266
  10.5 0.7 copy.267
  11.2 0.9 fusion.85
  12.1 0.9 fusion.87
  13.1 1.3 fusion.5.tok_ref
  14.4 0.7 pad_maximum_fusion.6.ow_ref
  16.8 1.0 pad_maximum_fusion.w_ref
  17.8 81.5 %gather_inputs.1 = (bf16[16,128,768]{2,1,0:T(8,128)(2,1)}, bf16[16,16,128]{2,1,0:T(8,128)(2,1)}, f32[4,8,256]{2,1,0:T(8,128)}, bf16[4,256,2048]{2,1,0:T(8,128)(2,1)}, bf16[4,128,1024]{2,1,0:T(8,128)(2,1)}) custom-call(bf16[4,128,768]{2,1,0:T(8,128)(2,1)} %pad_maximum_fusion.w_ref, bf16[4,16,128]{2,1,0:T(8,128)(2,1)} %pad.15.gt_ref, ...), custom_call_target="tpu_custom_call" | custom-call | bytes 100000000 | tf_op jit(solution)/shard_map/gather_inputs/pallas_call | solution.py:257
  99.3 0.8 copy_bitcast_fusion
  100.4 3.4 %fusion.27 = f32[4,1024]{1,0:T(4,128)S(1)} fusion(bf16[1024,2048]{1,0:T(8,128)(2,1)} %bitcast.242, bf16[2048,16]{0,1:T(8,128)(2,1)S(1)} %copy_bitcast_fusion, f32[4]{0:T(128)S(1)} %dynamic-slice_reduce_fusion), kind=kOutput, calls=%fused_computation.35 | convolution fusion | flops 16781312 | bytes 4227584 | tf_op jit(solution)/shard_map/dot_general | solution.py:553
  104.4 1.0 fusion.80
  105.9 6.9 %convolution_convert_fusion = bf16[1024,768]{1,0:T(8,128)(2,1)S(1)} fusion(bf16[1024,2048]{1,0:T(8,128)(2,1)} %bitcast.243, bf16[2048,768]{1,0:T(8,128)(2,1)} %bitcast.289), kind=kOutput, calls=%fused_computation.21 | convolution fusion | flops 3222011904 | bytes 8912896 | tf_op jit(solution)/shard_map/dot_general | solution.py:547
  112.8 1.3 bitcast_convert_fusion
  116.2 0.7 fusion.53.st_ref
  116.9 11.5 %exchange_states.1 = (f32[4,136,128]{2,1,0:T(8,128)}, bf16[2,128,128]{2,1,0:T(8,128)(2,1)}) custom-call(f32[2,136,128]{2,1,0:T(8,128)} %fusion.53.st_ref, bf16[1024,128]{1,0:T(8,128)(2,1)} %get-tuple-element.35.kv_ref), custom_call_target="tpu_custom_call" | custom-call | bytes 10000000 | tf_op jit(solution)/shard_map/exchange_states/pallas_call | solution.py:364
  128.4 1.0 select_bitcast_fusion
  130.8 0.7 slice_bitcast_fusion.9
  131.5 0.7 fusion.52
  132.2 0.7 broadcast_add_fusion
  133.6 1.3 multiply_reduce_fusion
  135.3 0.7 copy.229
  136.0 0.7 copy.230
  136.7 0.7 copy.231
  137.4 0.7 copy.232
  138.2 0.8 copy.196
  138.9 0.8 copy.198
  139.7 0.8 copy.200
  140.4 1.4 fusion.31
  142.1 0.7 slice.247
  142.8 1.2 copy.174
  144.0 0.7 fusion.10
  144.7 0.7 subtract_exponential_fusion.1
  146.2 1.1 multiply_reduce_fusion.1
  147.4 2.2 %fusion.18 = f32[2,1,4,256,128]{3,4,0,2,1:T(8,128)S(1)} fusion(bf16[4,256,128,1]{2,1,3,0:T(8,128)(2,1)S(1)} %bitcast.251, f32[2,4,256]{2,0,1:T(2,128)S(1)} %get-tuple-element.27, f32[2,4,256]{2,0,1:T(2,128)S(1)} %copy.179, f32[2,4,256]{2,0,1:T(2,128)S(1)} %copy-done.13, f32[4,256,256]{2,1,0:T(8,128)S(1)} %convolution_multiply_fusion, ...), kind=kOutput, calls=%fused_computation.25 | convolution fusion | flops 807927808 | bytes 2514944 | tf_op jit(solution)/shard_map/dhcts,hcsv->dhctv/dot_general | solution.py:644
  149.6 0.7 fusion.23
  153.2 0.7 fusion.2
  154.0 0.7 fusion
  154.8 0.9 fusion.43
  157.0 0.8 dynamic_slice.10
  157.7 1.2 multiply_reduce_fusion.5
  158.9 1.2 multiply_convert_fusion
  160.1 0.9 pad_maximum_fusion.3.mx_ref
  161.0 17.8 %exchange_mixed.1 = (bf16[8,256,256]{2,1,0:T(8,128)(2,1)}, f32[4,8,256]{2,1,0:T(8,128)}) custom-call(bf16[4,256,256]{2,1,0:T(8,128)(2,1)} %pad_maximum_fusion.3.mx_ref, f32[4,8,256]{2,1,0:T(8,128)} %pad.18.lt_ref), custom_call_target="tpu_custom_call" | custom-call | bytes 10000000 | tf_op jit(solution)/shard_map/exchange_mixed/pallas_call | solution.py:415
  178.8 1.5 copy.214
  180.5 0.8 slice.276
  181.9 4.3 %convolution_convert_fusion.1 = bf16[256,1024]{1,0:T(8,128)(2,1)} fusion(bf16[256,2048]{0,1:T(8,128)(2,1)S(1)} %bitcast.253, bf16[2048,1024]{1,0:T(8,128)(2,1)} %all-gather.2.cloned.1.call-done), kind=kOutput, calls=%fused_computation.31 | convolution fusion | flops 1074003968 | bytes 5767168 | tf_op jit(solution)/shard_map/dot_general | solution.py:680
  (125 shorter events, 13.9 us)
Async XLA Ops:
  7.2 93.0 %copy-start = (f32[4,4]{1,0:T(4,128)S(1)}, f32[4,4]{1,0:T(4,128)}, u32[]{:S(2)}) copy-start(f32[4,4]{1,0:T(4,128)} %param.23) | copy-start | bytes 196
  7.2 5.9 %copy-start.2 = (bf16[256,2048]{1,0:T(8,128)(2,1)S(1)}, bf16[256,2048]{1,0:T(8,128)(2,1)}, u32[]{:S(2)}) copy-start(bf16[256,2048]{1,0:T(8,128)(2,1)} %param.16) | copy-start | bytes 3145732
  7.2 5.8 %copy-start.7 = (bf16[128,256]{1,0:T(8,128)(2,1)S(1)}, bf16[128,256]{1,0:T(8,128)(2,1)}, u32[]{:S(2)}) copy-start(bf16[128,256]{1,0:T(8,128)(2,1)} %param.27) | copy-start | bytes 196612
  7.2 5.8 %copy-start.6 = (bf16[128,256]{1,0:T(8,128)(2,1)S(1)}, bf16[128,256]{1,0:T(8,128)(2,1)}, u32[]{:S(2)}) copy-start(bf16[128,256]{1,0:T(8,128)(2,1)} %param.28) | copy-start | bytes 196612
  7.2 5.9 %copy-start.12 = (f32[2048]{0:T(1024)S(1)}, f32[2048]{0:T(1024)}, u32[]{:S(2)}) copy-start(f32[2048]{0:T(1024)} %param.17) | copy-start | bytes 24580
  7.2 174.7 %all-gather.2.cloned.1.call-start = ((), (), s32[]{:S(2)}) async-start(), calls=%async_computation | async-start | bytes 5242880 | tf_op jit(solution)/shard_map/all_gather | solution.py:535
  9.7 4.7 %copy-start.8 = (bf16[64,1024]{1,0:T(8,128)(2,1)S(1)}, bf16[64,1024]{1,0:T(8,128)(2,1)}, u32[]{:S(2)}) copy-start(bf16[64,1024]{1,0:T(8,128)(2,1)} %param.31) | copy-start | bytes 393220
  9.7 4.7 %copy-start.9 = (bf16[64,1024]{1,0:T(8,128)(2,1)S(1)}, bf16[64,1024]{1,0:T(8,128)(2,1)}, u32[]{:S(2)}) copy-start(bf16[64,1024]{1,0:T(8,128)(2,1)} %param.30) | copy-start | bytes 393220
  112.8 1.3 copy-start.3
  131.5 6.6 %copy-start.5 = (f32[129,128]{1,0:T(8,128)S(1)}, f32[129,128]{1,0:T(8,128)}, u32[]{:S(2)}) copy-start(f32[129,128]{1,0:T(8,128)} %get-tuple-element.43) | copy-start | bytes 198148
  141.9 3.9 %copy-start.4 = (bf16[1024,128]{1,0:T(8,128)(2,1)S(1)}, bf16[1024,128]{1,0:T(8,128)(2,1)}, u32[]{:S(2)}) copy-start(bf16[1024,128]{1,0:T(8,128)(2,1)} %get-tuple-element.37) | copy-start | bytes 786436
  141.9 5.4 %copy-start.10 = (f32[2,4,256]{2,1,0:T(4,128)S(1)}, f32[2,4,256]{2,1,0:T(4,128)}, u32[]{:S(2)}) copy-start(f32[2,4,256]{2,1,0:T(4,128)} %broadcast_add_fusion) | copy-start | bytes 24580
  141.9 5.4 %copy-start.13 = (f32[2,4,256]{2,0,1:T(2,128)S(1)}, f32[2,4,256]{2,0,1:T(2,128)}, u32[]{:S(2)}) copy-start(f32[2,4,256]{2,0,1:T(2,128)} %copy.177) | copy-start | bytes 24580
  150.3 0.8 copy-start.11
  150.3 1.0 copy-start.1
  150.4 1.8 copy-start.14
Sparse Core Ops, SparseCore 0:
  99.4 50.6 all-gather.1

commit v3 on v2

--- a/solution.py
+++ b/solution.py
@@ -159,7 +159,7 @@
                 def _():
                     down(k, d).start()
 
-            if d == g - 1:
+            if d == 0:
                 if k > 0:
 
                     @pl.when(q >= k)
@@ -376,42 +376,66 @@
     )(states, kv_pairs)
 
 
-def mix_kernel(g, tp, mx_ref, lt_ref, mx_out, lt_out, own_sem, mx_send, mx_recv, lt_send, lt_recv):
+def mix_kernel(
+    g, tp, mx_ref, lt_ref, mx_out, lt_out, own_sem, mx_send, mx_recv, fw_send, fw_recv, lt_send, lt_recv
+):
     me, c = lax.axis_index("sp"), lax.axis_index("tp")
     q, h = lax.div(me, g), lax.rem(me, g)
-    total = g * tp
-    mine = h * tp + c
-    peers = []
-    for k in range(1, total):
-        to = lax.rem(mine + k, total)
-        peers.append((lax.div(to, tp), lax.rem(to, tp)))
-    greet([{"sp": q * g + a, "tp": b} for a, b in peers])
-    copies = []
-    for k, (a, b) in enumerate(peers):
-        copies.append(
+    greet(
+        [{"sp": q * g + lax.rem(h + d, g)} for d in range(1, g)]
+        + [{"tp": lax.rem(c + e, tp)} for e in range(1, tp)]
+    )
+    copies, direct = [], []
+    for d in range(1, g):
+        a = lax.rem(h + d, g)
+        direct.append(
             remote(
-                mx_ref.at[a], mx_out.at[mine], mx_send.at[k], mx_recv.at[k], sp=q * g + a, tp=b
+                mx_ref.at[a],
+                mx_out.at[h * tp + c],
+                mx_send.at[d - 1],
+                mx_recv.at[d - 1],
+                sp=q * g + a,
             )
         )
-    for d in range(1, g):
-        a = lax.rem(h + d, g)
         copies.append(
             remote(lt_ref.at[a], lt_out.at[h], lt_send.at[d - 1], lt_recv.at[d - 1], sp=q * g + a)
         )
-    own = [
-        pltpu.make_async_copy(mx_ref.at[h], mx_out.at[mine], own_sem.at[0]),
-        pltpu.make_async_copy(lt_ref.at[h], lt_out.at[h], own_sem.at[1]),
-    ]
-    for copy in copies + own:
+    copies.append(pltpu.make_async_copy(mx_ref.at[h], mx_out.at[h * tp + c], own_sem.at[0]))
+    copies.append(pltpu.make_async_copy(lt_ref.at[h], lt_out.at[h], own_sem.at[1]))
+    for copy in direct:
         copy.start()
-    for copy in copies + own:
+
+    def pass_on(d, e):
+        slot = lax.rem(h - d + g, g) * tp + c
+        src = mx_ref.at[h] if d == 0 else mx_out.at[slot]
+        return remote(
+            src,
+            mx_out.at[slot],
+            fw_send.at[d, e - 1],
+            fw_recv.at[d, e - 1],
+            tp=lax.rem(c + e, tp),
+        )
+
+    for e in range(1, tp):
+        copies.append(pass_on(0, e))
+    for copy in copies:
+        copy.start()
+    for d in range(1, g):
+        direct[d - 1].wait_recv()
+        for e in range(1, tp):
+            copy = pass_on(d, e)
+            copy.start()
+            copies.append(copy)
+    for copy in direct:
+        copy.wait_send()
+    for copy in copies:
         copy.wait()
 
 
 def exchange_mixed(g, tp, mixed, logs):
     vmem = pl.BlockSpec(memory_space=pltpu.VMEM)
     dma = pltpu.SemaphoreType.DMA
-    few, many = max(g - 1, 1), max(g * tp - 1, 1)
+    few, cores = max(g - 1, 1), max(tp - 1, 1)
     return pl.pallas_call(
         functools.partial(mix_kernel, g, tp),
         name="exchange_mixed",
@@ -421,7 +445,15 @@
         ),
         in_specs=[vmem] * 2,
         out_specs=(vmem,) * 2,
-        scratch_shapes=[dma((2,)), dma((many,)), dma((many,)), dma((few,)), dma((few,))],
+        scratch_shapes=[
+            dma((2,)),
+            dma((few,)),
+            dma((few,)),
+            dma((g, cores)),
+            dma((g, cores)),
+            dma((few,)),
+            dma((few,)),
+        ],
         compiler_params=pltpu.CompilerParams(collective_id=2, has_side_effects=True),
         cost_estimate=pl.CostEstimate(flops=0, bytes_accessed=10_000_000, transcendentals=0),
     )(mixed, logs)

time: 194 us -> 185 us (0.954)
  Pallas kernels: 111 us -> 102 us
    pallas_call x1, Pallas kernels: 17.8 us -> 11.4 us  [exchange_mixed(): pl.pallas_call(functools.partial(mix_kernel, g, tp), name='exchange_mixed...]
    pallas_call x1, Pallas kernels: 81.5 us -> 79.3 us  [gather_inputs(): pl.pallas_call(functools.partial(gather_kernel, n, g), name='gather_input...]
  transfers between devices with their start and end apart: 1 -> 1, of which waited for: 0 -> 0; matrix products, arithmetic and copies ran while one was open for 27% -> 28% of each run, Pallas kernels for 15% -> 12%
where the time goes in v3:
time: 185 us; the launch traced here: 184 us
  Pallas kernels  102 us (55%)
  local copies, waits for them, and re-layouts  24.1 us (13%)
  other arithmetic  22.1 us (12%)
  matrix products  20.9 us (11%)
  between operations  14.7 us (8%)
    pallas_call x1, Pallas kernels, gather_inputs(): pl.pallas_call(functools.partial(gather_kernel, n, g), name='gather_input...  79.3 us
    pallas_call x1, Pallas kernels, exchange_states(): pl.pallas_call(functools.partial(state_kernel, ng, g), name='exchange_sta...  11.5 us
    pallas_call x1, Pallas kernels, exchange_mixed(): pl.pallas_call(functools.partial(mix_kernel, g, tp), name='exchange_mixed...  11.4 us
    dot_general x1, matrix products, on_device(): jnp.dot(tok_all, w_all, preferred_element_type=jnp.float32)  6.59 us
    mul x9, local copies, waits for them, and re-layouts, on_device(): state = state + scale[..., g + o, None, None] * outer_sum[o][None, :, None]  5.76 us
    dot_general x1, matrix products, on_device(): mixed = jnp.dot(full, out_w, preferred_element_type=jnp.float32)  4.25 us
  transfers between devices with their start and end apart: 1, of which 0 were waited for; matrix products, arithmetic and copies ran while one was open for 28% of the time, Pallas kernels for 12%

profile of v3, /device:TPU:0, one launch (start us, length us, event | category | flops | bytes accessed | tf_op | source)
XLA Modules:
  0.0 184.1 jit_solution(15903700706925061777)
XLA Ops:
  7.3 0.9 fusion.89
  8.2 1.5 fusion.3
  9.7 0.8 copy.266
  10.5 0.7 copy.267
  11.2 0.9 fusion.85
  12.1 0.9 fusion.87
  13.1 1.3 fusion.5.tok_ref
  14.4 0.7 pad_maximum_fusion.6.ow_ref
  16.8 1.0 pad_maximum_fusion.w_ref
  17.8 79.3 %gather_inputs.1 = (bf16[16,128,768]{2,1,0:T(8,128)(2,1)}, bf16[16,16,128]{2,1,0:T(8,128)(2,1)}, f32[4,8,256]{2,1,0:T(8,128)}, bf16[4,256,2048]{2,1,0:T(8,128)(2,1)}, bf16[4,128,1024]{2,1,0:T(8,128)(2,1)}) custom-call(bf16[4,128,768]{2,1,0:T(8,128)(2,1)} %pad_maximum_fusion.w_ref, bf16[4,16,128]{2,1,0:T(8,128)(2,1)} %pad.15.gt_ref, ...), custom_call_target="tpu_custom_call" | custom-call | bytes 100000000 | tf_op jit(solution)/shard_map/gather_inputs/pallas_call | solution.py:257
  97.2 0.8 copy_bitcast_fusion
  98.2 3.4 %fusion.27 = f32[4,1024]{1,0:T(4,128)S(1)} fusion(bf16[1024,2048]{1,0:T(8,128)(2,1)} %bitcast.242, bf16[2048,16]{0,1:T(8,128)(2,1)S(1)} %copy_bitcast_fusion, f32[4]{0:T(128)S(1)} %dynamic-slice_reduce_fusion), kind=kOutput, calls=%fused_computation.35 | convolution fusion | flops 16781312 | bytes 4227584 | tf_op jit(solution)/shard_map/dot_general | solution.py:585
  102.2 1.0 fusion.80
  103.7 6.6 %convolution_convert_fusion = bf16[1024,768]{1,0:T(8,128)(2,1)S(1)} fusion(bf16[1024,2048]{1,0:T(8,128)(2,1)} %bitcast.243, bf16[2048,768]{1,0:T(8,128)(2,1)} %bitcast.289), kind=kOutput, calls=%fused_computation.21 | convolution fusion | flops 3222011904 | bytes 8912896 | tf_op jit(solution)/shard_map/dot_general | solution.py:579
  110.4 1.3 bitcast_convert_fusion
  113.8 0.7 fusion.53.st_ref
  114.4 11.5 %exchange_states.1 = (f32[4,136,128]{2,1,0:T(8,128)}, bf16[2,128,128]{2,1,0:T(8,128)(2,1)}) custom-call(f32[2,136,128]{2,1,0:T(8,128)} %fusion.53.st_ref, bf16[1024,128]{1,0:T(8,128)(2,1)} %get-tuple-element.35.kv_ref), custom_call_target="tpu_custom_call" | custom-call | bytes 10000000 | tf_op jit(solution)/shard_map/exchange_states/pallas_call | solution.py:364
  125.9 1.0 select_bitcast_fusion
  128.3 0.7 slice_bitcast_fusion.9
  129.0 0.7 fusion.52
  129.7 0.7 broadcast_add_fusion
  131.1 1.3 multiply_reduce_fusion
  132.8 0.7 copy.229
  133.5 0.7 copy.230
  134.2 0.7 copy.231
  134.9 0.7 copy.232
  135.7 0.8 copy.196
  136.4 0.8 copy.198
  137.2 0.8 copy.200
  137.9 1.4 fusion.31
  139.6 0.7 slice.247
  140.3 1.2 copy.174
  141.5 0.7 fusion.10
  142.2 0.7 subtract_exponential_fusion.1
  143.7 1.1 multiply_reduce_fusion.1
  144.9 2.2 %fusion.18 = f32[2,1,4,256,128]{3,4,0,2,1:T(8,128)S(1)} fusion(bf16[4,256,128,1]{2,1,3,0:T(8,128)(2,1)S(1)} %bitcast.251, f32[2,4,256]{2,0,1:T(2,128)S(1)} %get-tuple-element.27, f32[2,4,256]{2,0,1:T(2,128)S(1)} %copy.179, f32[2,4,256]{2,0,1:T(2,128)S(1)} %copy-done.13, f32[4,256,256]{2,1,0:T(8,128)S(1)} %convolution_multiply_fusion, ...), kind=kOutput, calls=%fused_computation.25 | convolution fusion | flops 807927808 | bytes 2514944 | tf_op jit(solution)/shard_map/dhcts,hcsv->dhctv/dot_general | solution.py:676
  147.1 0.7 fusion.23
  150.6 0.7 fusion.2
  151.5 0.7 fusion
  152.3 0.9 fusion.43
  154.5 0.8 dynamic_slice.10
  155.2 1.2 multiply_reduce_fusion.5
  156.4 1.2 multiply_convert_fusion
  157.6 0.9 pad_maximum_fusion.3.mx_ref
  158.4 11.4 %exchange_mixed.1 = (bf16[8,256,256]{2,1,0:T(8,128)(2,1)}, f32[4,8,256]{2,1,0:T(8,128)}) custom-call(bf16[4,256,256]{2,1,0:T(8,128)(2,1)} %pad_maximum_fusion.3.mx_ref, f32[4,8,256]{2,1,0:T(8,128)} %pad.18.lt_ref), custom_call_target="tpu_custom_call" | custom-call | bytes 10000000 | tf_op jit(solution)/shard_map/exchange_mixed/pallas_call | solution.py:439
  169.9 1.5 copy.214
  171.6 0.8 slice.276
  173.0 4.3 %convolution_convert_fusion.1 = bf16[256,1024]{1,0:T(8,128)(2,1)} fusion(bf16[256,2048]{0,1:T(8,128)(2,1)S(1)} %bitcast.253, bf16[2048,1024]{1,0:T(8,128)(2,1)} %all-gather.2.cloned.1.call-done), kind=kOutput, calls=%fused_computation.31 | convolution fusion | flops 1074003968 | bytes 5767168 | tf_op jit(solution)/shard_map/dot_general | solution.py:712
  (125 shorter events, 13.9 us)
Async XLA Ops:
  7.2 90.9 %copy-start = (f32[4,4]{1,0:T(4,128)S(1)}, f32[4,4]{1,0:T(4,128)}, u32[]{:S(2)}) copy-start(f32[4,4]{1,0:T(4,128)} %param.23) | copy-start | bytes 196
  7.2 5.9 %copy-start.2 = (bf16[256,2048]{1,0:T(8,128)(2,1)S(1)}, bf16[256,2048]{1,0:T(8,128)(2,1)}, u32[]{:S(2)}) copy-start(bf16[256,2048]{1,0:T(8,128)(2,1)} %param.16) | copy-start | bytes 3145732
  7.2 5.8 %copy-start.7 = (bf16[128,256]{1,0:T(8,128)(2,1)S(1)}, bf16[128,256]{1,0:T(8,128)(2,1)}, u32[]{:S(2)}) copy-start(bf16[128,256]{1,0:T(8,128)(2,1)} %param.27) | copy-start | bytes 196612
  7.2 5.8 %copy-start.6 = (bf16[128,256]{1,0:T(8,128)(2,1)S(1)}, bf16[128,256]{1,0:T(8,128)(2,1)}, u32[]{:S(2)}) copy-start(bf16[128,256]{1,0:T(8,128)(2,1)} %param.28) | copy-start | bytes 196612
  7.2 5.9 %copy-start.12 = (f32[2048]{0:T(1024)S(1)}, f32[2048]{0:T(1024)}, u32[]{:S(2)}) copy-start(f32[2048]{0:T(1024)} %param.17) | copy-start | bytes 24580
  7.2 165.8 %all-gather.2.cloned.1.call-start = ((), (), s32[]{:S(2)}) async-start(), calls=%async_computation | async-start | bytes 5242880 | tf_op jit(solution)/shard_map/all_gather | solution.py:567
  9.7 4.7 %copy-start.8 = (bf16[64,1024]{1,0:T(8,128)(2,1)S(1)}, bf16[64,1024]{1,0:T(8,128)(2,1)}, u32[]{:S(2)}) copy-start(bf16[64,1024]{1,0:T(8,128)(2,1)} %param.31) | copy-start | bytes 393220
  9.7 4.7 %copy-start.9 = (bf16[64,1024]{1,0:T(8,128)(2,1)S(1)}, bf16[64,1024]{1,0:T(8,128)(2,1)}, u32[]{:S(2)}) copy-start(bf16[64,1024]{1,0:T(8,128)(2,1)} %param.30) | copy-start | bytes 393220
  110.3 1.3 copy-start.3
  129.0 6.6 %copy-start.5 = (f32[129,128]{1,0:T(8,128)S(1)}, f32[129,128]{1,0:T(8,128)}, u32[]{:S(2)}) copy-start(f32[129,128]{1,0:T(8,128)} %get-tuple-element.43) | copy-start | bytes 198148
  139.3 3.9 %copy-start.4 = (bf16[1024,128]{1,0:T(8,128)(2,1)S(1)}, bf16[1024,128]{1,0:T(8,128)(2,1)}, u32[]{:S(2)}) copy-start(bf16[1024,128]{1,0:T(8,128)(2,1)} %get-tuple-element.37) | copy-start | bytes 786436
  139.4 5.4 %copy-start.10 = (f32[2,4,256]{2,1,0:T(4,128)S(1)}, f32[2,4,256]{2,1,0:T(4,128)}, u32[]{:S(2)}) copy-start(f32[2,4,256]{2,1,0:T(4,128)} %broadcast_add_fusion) | copy-start | bytes 24580
  139.4 5.4 %copy-start.13 = (f32[2,4,256]{2,0,1:T(2,128)S(1)}, f32[2,4,256]{2,0,1:T(2,128)}, u32[]{:S(2)}) copy-start(f32[2,4,256]{2,0,1:T(2,128)} %copy.177) | copy-start | bytes 24580
  147.8 0.8 copy-start.11
  147.8 1.0 copy-start.1
  147.9 1.8 copy-start.14
Sparse Core Ops, SparseCore 0:
  97.2 49.7 all-gather.1
